TPU v7x, 256 devices: a whole 4x4x8 slice. The times are simulated.
256 devices in a mesh: ep: 64 (over z, x, core), tp: 4 (over y).
Axes of the slice: x: 4, y: 4, z: 8, core: 2. Of those that a mesh axis runs over, the one named last changes fastest.
Arguments:
- mix_in: bfloat16 [8192, 2048], P('ep'), may hold values from -6 to 6
- mix_gain: float32 [2048], replicated, may hold values from 0.1 to 1.9
- query_weight: bfloat16 [2048, 3072], P(None, 'tp'), may hold values from -0.125 to 0.125
- latent_weight: bfloat16 [2048, 512], replicated, may hold values from -0.125 to 0.125
- rotary_weight: bfloat16 [2048, 64], replicated, may hold values from -0.125 to 0.125
- latent_gain: float32 [512], replicated, may hold values from 0.1 to 1.9
- key_weight: bfloat16 [512, 2048], P(None, 'tp'), may hold values from -0.25 to 0.25
- value_weight: bfloat16 [512, 2048], P(None, 'tp'), may hold values from -0.25 to 0.25
- output_weight: bfloat16 [2048, 2048], P('tp'), may hold values from -0.125 to 0.125
- out_gain: float32 [2048], replicated, may hold values from 0.1 to 1.9
- ffn_in: bfloat16 [8192, 2048], P('ep'), may hold values from -6 to 6
- ffn_gain: float32 [2048], replicated, may hold values from 0.1 to 1.9
- gate_weight: bfloat16 [64, 2048, 1024], P('ep', None, 'tp'), may hold values from -0.375 to 0.375
- up_weight: bfloat16 [64, 2048, 1024], P('ep', None, 'tp'), may hold values from -0.375 to 0.375
- down_weight: bfloat16 [64, 1024, 2048], P('ep', 'tp'), may hold values from -0.046875 to 0.046875
- routes: int32 [8192, 4], P('ep'), may hold values from 0 to 63, all different within a row; in each aligned block of 32 rows (0 to 31, 32 to 63, ...) at most 4 rows name the same one
- route_scores: float32 [8192, 4], P('ep'), may hold values from -6 to 6
Outputs:
- mixed: bfloat16 [8192, 2048], P(('ep', 'tp'))
- moe_out: bfloat16 [8192, 2048], P(('ep', 'tp'))
Inputs may be any that keep to these rules, and one draw needn't show every extreme that they name: `routes`: each row names 4 different experts; in each aligned block of 32 rows no expert is named by more than 4 rows, a bound that some blocks reach.
All inputs are finite; a program needn't handle non-finite values.
Results may differ from a plain program's by a relative error of at most 0.014.
Values may be sent and summed in bfloat16 or wider, within the bound.
A program may use at most 192 MiB of HBM per device.

v0:
```python
import jax
import jax.numpy as jnp
import numpy as np
from jax import lax
from jax.experimental import pallas as pl
from jax.experimental.pallas import tpu as pltpu
from jax.sharding import PartitionSpec as P

NOPE = 128
ROPE = 64
VD = 128
QB = 32
MOST = 4

norm_eps = 1e-06
clamp_limit = 7.0
gate_slope = 1.702
rope_base = 10000.0

MESH = pl.DeviceIdType.MESH
bf16 = jnp.bfloat16
f32 = jnp.float32

ORDER = (0, 1, 7, 2, 6, 3, 5, 4)


def iota(shape, dim):
    return lax.broadcasted_iota(jnp.int32, shape, dim)


def rms(rows, gain):
    mean_square = jnp.mean(rows * rows, axis=-1, keepdims=True)
    return rows * lax.rsqrt(mean_square + norm_eps) * gain


def drain(view, sem):
    pltpu.make_async_copy(view, view, sem).wait()


def kernel(
    NZ,
    J,
    TP,
    mix_in,
    mix_gain,
    query_weight,
    latent_weight,
    rotary_weight,
    latent_gain,
    key_weight,
    value_weight,
    output_weight,
    out_gain,
    ffn_in,
    ffn_gain,
    gate_weight,
    up_weight,
    down_weight,
    routes,
    route_scores,
    base_turn,
    row_turn,
    mixed_out,
    moe_out,
    mix_v,
    ffn_v,
    qw,
    lw,
    rw,
    kw,
    vw,
    ow,
    gw,
    uw,
    wd,
    outg,
    X,
    H,
    Dn,
    R,
    sel,
    w_hi,
    w_lo,
    m_send,
    m_recv,
    Q,
    KV,
    q_out,
    kv_out,
    Kc,
    Vc,
    o_out,
    t_out,
    o_in,
    t_in,
    p_out,
    p_in,
    load_sem,
    disp_recv,
    x_recv,
    h_recv,
    one_recv,
    send_sem,
):
    E = NZ * J
    e = lax.axis_index("ep")
    t = lax.axis_index("tp")
    z = e // J
    j = e % J
    rows = ffn_v.shape[0]
    width = outg.shape[1]
    cell = outg.shape[0] // E
    right = lax.rem(t + 1, TP)
    left = lax.rem(t + TP - 1, TP)
    unit = J * cell

    def load(src, dst, number):
        copy = pltpu.make_async_copy(src, dst, load_sem.at[number])
        copy.start()
        return copy

    def send(src, dst, s_sem, r_sem, ep, tp):
        pltpu.make_async_remote_copy(
            src_ref=src,
            dst_ref=dst,
            send_sem=s_sem,
            recv_sem=r_sem,
            device_id=(ep, tp),
            device_id_type=MESH,
        ).start()

    load_ffn = load(ffn_in, ffn_v, 0)
    load_mix = load(mix_in, mix_v, 1)
    load_q = load(query_weight, qw, 2)
    load_l = load(latent_weight, lw, 3)
    load_r = load(rotary_weight, rw, 4)
    load_k = load(key_weight, kw, 5)
    load_v = load(value_weight, vw, 6)
    load_g = load(gate_weight.at[0], gw, 7)
    load_u = load(up_weight.at[0], uw, 8)
    load_d = load(
        down_weight.at[0, :, pl.ds(pl.multiple_of(t * width, 128), width)], wd.at[t], 9
    )
    load_o = load(output_weight, ow, 10)

    barrier = pltpu.get_barrier_semaphore()

    @pl.loop(1, E)
    def _(step):
        pl.semaphore_signal(
            barrier, inc=1, device_id=(lax.rem(e + step, E), t), device_id_type=MESH
        )

    for step in range(1, TP):
        pl.semaphore_signal(
            barrier, inc=1, device_id=(e, lax.rem(t + step, TP)), device_id_type=MESH
        )

    slots = outg.shape[0]
    blocks = rows // QB
    slot = iota((1, slots), 1)
    slot_expert = slot // cell
    slot_block = (slot // MOST) % blocks
    slot_rank = (slot % MOST).astype(f32)
    row_block = iota((rows, 1), 0) // QB
    route = routes[...]
    choose = route.shape[1]
    named = jnp.zeros((rows, slots), f32)
    for k in range(choose):
        named = named + jnp.where(route[:, k : k + 1] == slot_expert, 1.0, 0.0)
    low_r = iota((rows, rows), 0)
    low_c = iota((rows, rows), 1)
    lower = jnp.where((low_c < low_r) & (low_c // QB == low_r // QB), 1.0, 0.0).astype(bf16)
    rank = jnp.dot(lower, named.astype(bf16), preferred_element_type=f32)
    picked = jnp.where((rank == slot_rank) & (row_block == slot_block), named, 0.0)
    sel[...] = picked.astype(bf16)

    load_ffn.wait()
    x = ffn_v[...].astype(f32)
    inverse = lax.rsqrt(jnp.mean(x * x, axis=-1, keepdims=True) + norm_eps)
    columns = pl.ds(pl.multiple_of(t * width, 128), width)
    normed_part = (ffn_v[:, columns].astype(f32) * inverse * ffn_gain[:, columns]).astype(bf16)
    outg[...] = lax.dot_general(
        sel[...], normed_part, (((0,), (0,)), ((), ())), preferred_element_type=f32
    ).astype(bf16)

    pl.semaphore_wait(barrier, E - 1 + TP - 1)

    my_rows = pl.ds(pl.multiple_of(e * cell, cell), cell)
    for number, dz in enumerate(ORDER):
        target_z = lax.rem(z + NZ - dz, NZ)

        @pl.loop(1 if dz == 0 else 0, J)
        def _(step, number=number, target_z=target_z):
            target = target_z * J + lax.rem(j + step, J)
            send(
                outg.at[pl.ds(pl.multiple_of(target * cell, cell), cell)],
                X.at[t, my_rows],
                send_sem.at[0],
                disp_recv.at[number],
                target,
                t,
            )

    X[t, my_rows] = outg[my_rows, :]

    for step in range(1, TP):
        peer = lax.rem(t + step, TP)
        send(
            down_weight.at[0, :, pl.ds(pl.multiple_of(peer * width, 128), width)],
            wd.at[t],
            send_sem.at[1],
            one_recv.at[0],
            e,
            peer,
        )

    load_mix.wait()
    normed = rms(mix_v[...].astype(f32), mix_gain[...]).astype(bf16)
    load_q.wait()
    queries = jnp.dot(normed, qw[...], preferred_element_type=f32)
    base = base_turn[pl.ds(e, 1), :]
    base_cos, base_sin = base[:, :128], base[:, 128:]
    row_cos, row_sin = row_turn[:, :128], row_turn[:, 128:]
    cosine = base_cos * row_cos - base_sin * row_sin
    sine = base_sin * row_cos + base_cos * row_sin
    lane = iota((rows, 128), 1)
    first_half = lane % ROPE < ROPE // 2
    sine = jnp.where(first_half, -sine, sine)

    def turned(v):
        partner = jnp.where(first_half, pltpu.roll(v, 96, 1), pltpu.roll(v, 32, 1))
        return v * cosine + partner * sine

    low_lanes = lane < 64
    A = [queries[:, 128 * i : 128 * (i + 1)] for i in range(6)]
    q_out[:, 0:128] = A[0].astype(bf16)
    q_out[:, 128:256] = pltpu.roll(jnp.where(low_lanes, A[2], A[1]), 64, 1).astype(bf16)
    q_out[:, 256:384] = A[3].astype(bf16)
    q_out[:, 384:512] = pltpu.roll(jnp.where(low_lanes, A[5], A[4]), 64, 1).astype(bf16)
    q_out[:, 512:640] = turned(jnp.where(low_lanes, A[1], A[2])).astype(bf16)
    q_out[:, 640:768] = turned(jnp.where(low_lanes, A[4], A[5])).astype(bf16)

    load_l.wait()
    latent = jnp.dot(normed, lw[...], preferred_element_type=f32)
    kv_out[:, 0:512] = rms(latent, latent_gain[...]).astype(bf16)
    load_r.wait()
    rotary = jnp.dot(normed, rw[...], preferred_element_type=f32)
    kv_out[:, 512:640] = turned(jnp.concatenate([rotary, rotary], axis=1)).astype(bf16)

    for step in range(1, J):
        send(
            q_out,
            Q.at[j],
            send_sem.at[2],
            one_recv.at[1],
            z * J + lax.rem(j + step, J),
            t,
        )
    for step in (1, 7, 2, 6, 3, 5, 4):
        send(
            kv_out,
            KV.at[z],
            send_sem.at[3],
            one_recv.at[2],
            lax.rem(z + step, NZ) * J + j,
            t,
        )
    Q[j] = q_out[...]
    KV[z] = kv_out[...]

    score = route_scores[...]
    grown = jnp.exp(score - jnp.max(score, axis=-1, keepdims=True))
    share = grown / jnp.sum(grown, axis=-1, keepdims=True)
    gates = jnp.zeros((rows, slots), f32)
    for k in range(choose):
        gates = gates + jnp.where(route[:, k : k + 1] == slot_expert, share[:, k : k + 1], 0.0)
    gates = gates * sel[...].astype(f32)
    gates_hi = gates.astype(bf16)
    w_hi[...] = gates_hi
    w_lo[...] = (gates - gates_hi.astype(f32)).astype(bf16)

    def unit_rows(number):
        source_z = lax.rem(z + ORDER[number], NZ)
        return pl.ds(pl.multiple_of(source_z * unit, unit), unit)

    def spread(buf, number, sems, base_send):
        place = unit_rows(number)
        send(buf.at[t, place], buf.at[t, place], send_sem.at[base_send], sems.at[0, number], e, right)
        send(buf.at[t, place], buf.at[t, place], send_sem.at[base_send], sems.at[1, number], e, left)

    def relay(buf, number, sems, base_send):
        place = unit_rows(number)
        drain(buf.at[left, place], sems.at[0, number])
        drain(buf.at[right, place], sems.at[1, number])
        if number % 2 == 0:
            send(
                buf.at[left, place],
                buf.at[left, place],
                send_sem.at[base_send + 1],
                sems.at[2, number],
                e,
                right,
            )
        else:
            send(
                buf.at[right, place],
                buf.at[right, place],
                send_sem.at[base_send + 1],
                sems.at[2, number],
                e,
                left,
            )

    def relayed(buf, number, sems):
        across = lax.rem(t + 2, TP)
        drain(buf.at[across, unit_rows(number)], sems.at[2, number])

    def take(number):
        if ORDER[number] == 0:
            drain(X.at[t, pl.ds(0, unit - cell)], disp_recv.at[number])
        else:
            drain(X.at[t, pl.ds(0, unit)], disp_recv.at[number])
        spread(X, number, x_recv, 4)

    def hidden(batch):
        pair = (2 * batch, 2 * batch + 1)
        for number in pair:
            relayed(X, number, x_recv)
        gate_part = jnp.zeros((2 * unit, gw.shape[1]), f32)
        up_part = jnp.zeros((2 * unit, gw.shape[1]), f32)
        for part in range(TP):
            block = jnp.concatenate([X[part, unit_rows(number)] for number in pair], axis=0)
            depth = pl.ds(part * width, width)
            gate_part = gate_part + jnp.dot(block, gw[depth, :], preferred_element_type=f32)
            up_part = up_part + jnp.dot(block, uw[depth, :], preferred_element_type=f32)
        gate_part = jnp.minimum(gate_part, clamp_limit)
        up_part = jnp.clip(up_part, -clamp_limit, clamp_limit)
        result = (gate_part * jax.nn.sigmoid(gate_slope * gate_part) * (up_part + 1.0)).astype(bf16)
        for i, number in enumerate(pair):
            H[t, unit_rows(number)] = result[i * unit : (i + 1) * unit]
        for number in pair:
            spread(H, number, h_recv, 6)

    def hidden_relay(batch):
        for number in (2 * batch, 2 * batch + 1):
            relay(H, number, h_recv, 6)

    def down(batch):
        pair = (2 * batch, 2 * batch + 1)
        for number in pair:
            relayed(H, number, h_recv)
        total = jnp.zeros((2 * unit, width), f32)
        for part in range(TP):
            block = jnp.concatenate([H[part, unit_rows(number)] for number in pair], axis=0)
            total = total + jnp.dot(block, wd[part], preferred_element_type=f32)
        total = total.astype(bf16)
        for i, number in enumerate(pair):
            Dn[unit_rows(number), :] = total[i * unit : (i + 1) * unit]
        for number in pair:
            source_z = lax.rem(z + ORDER[number], NZ)

            @pl.loop(1 if ORDER[number] == 0 else 0, J)
            def _(step, source_z=source_z):
                source = source_z * J + lax.rem(j + step, J)
                send(
                    Dn.at[pl.ds(pl.multiple_of(source * cell, cell), cell)],
                    R.at[my_rows],
                    send_sem.at[8],
                    one_recv.at[3],
                    source,
                    t,
                )

            if ORDER[number] == 0:
                R[my_rows, :] = Dn[my_rows, :]

    def expand():
        drain(Q.at[pl.ds(0, J - 1)], one_recv.at[1])
        drain(KV.at[pl.ds(0, NZ - 1)], one_recv.at[2])
        load_k.wait()
        load_v.wait()
        lat = KV[...].reshape(NZ * rows, 640)
        turn = lat[:, 512:640]
        keys = jnp.dot(lat[:, :512], kw[...], preferred_element_type=f32).astype(bf16)
        values = jnp.dot(lat[:, :512], vw[...], preferred_element_type=f32).astype(bf16)
        low = iota((NZ * rows, 128), 1) < 64
        zero = jnp.zeros_like(turn)
        even, odd = jnp.where(low, turn, zero), jnp.where(low, zero, turn)
        ones = jnp.ones_like(turn)
        for h in range(4):
            Kc[h, :, 0:128] = keys[:, 128 * h : 128 * (h + 1)]
            Kc[h, :, 128:256] = even if h % 2 == 0 else odd
            Vc[h, :, 0:128] = values[:, 128 * h : 128 * (h + 1)]
            Vc[h, :, 128:256] = ones

    scale = (NOPE + ROPE) ** (-0.5)

    def head(h):
        span = 2 * rows

        @pl.loop(0, J // 2)
        def _(chunk):
            plain = Q[pl.ds(2 * chunk, 2), :, 128 * h : 128 * (h + 1)].reshape(span, 128)
            pair = 512 + 128 * (h // 2)
            turn = Q[pl.ds(2 * chunk, 2), :, pair : pair + 128].reshape(span, 128)
            both = jnp.concatenate([plain, turn], axis=1)
            scores = lax.dot_general(
                both, Kc[h], (((1,), (1,)), ((), ())), preferred_element_type=f32
            )
            place = iota((1, NZ * rows), 1)
            key_place = (place // rows) * (J * rows) + j * rows + place % rows
            query_place = z * (J * rows) + chunk * span + iota((span, 1), 0)
            weights = jnp.where(key_place <= query_place, jnp.exp(scores * scale), 0.0).astype(bf16)
            both_out = jnp.dot(weights, Vc[h], preferred_element_type=f32)
            here = pl.ds(pl.multiple_of(chunk * span, span), span)
            o_out[here, 128 * h : 128 * (h + 1)] = both_out[:, :128].astype(bf16)
            sums = both_out[:, 128:]
            if h == 0:
                t_out[here, :] = sums
            else:
                lanes = iota((span, 128), 1)
                t_out[here, :] = jnp.where(lanes // 32 == h, sums, t_out[here, :])

    def give_back():
        for step in range(1, J):
            target = lax.rem(j + step, J)
            place = pl.ds(pl.multiple_of(target * rows, rows), rows)
            send(o_out.at[place], o_in.at[j], send_sem.at[9], one_recv.at[4], z * J + target, t)
            send(t_out.at[place], t_in.at[j], send_sem.at[10], one_recv.at[5], z * J + target, t)
        place = pl.ds(pl.multiple_of(j * rows, rows), rows)
        o_in[j] = o_out[place, :]
        t_in[j] = t_out[place, :]

    quarter = rows // TP

    def project():
        drain(o_in.at[pl.ds(0, J - 1)], one_recv.at[4])
        drain(t_in.at[pl.ds(0, J - 1)], one_recv.at[5])
        load_o.wait()
        osum = jnp.zeros((rows, 4 * VD), f32)
        tsum = jnp.zeros((rows, 128), f32)
        for i in range(J):
            osum = osum + o_in[i].astype(f32)
            tsum = tsum + t_in[i]
        heads = [
            (osum[:, VD * h : VD * (h + 1)] / tsum[:, 32 * h : 32 * h + 1]).astype(bf16)
            for h in range(4)
        ]
        attended = jnp.concatenate(heads, axis=1)
        p_out[...] = jnp.dot(attended, ow[...], preferred_element_type=f32).astype(bf16)
        for step in range(1, TP):
            peer = lax.rem(t + step, TP)
            place = pl.ds(pl.multiple_of(peer * quarter, quarter), quarter)
            send(p_out.at[place], p_in.at[t], send_sem.at[11], one_recv.at[6], e, peer)
        p_in[t] = p_out[pl.ds(pl.multiple_of(t * quarter, quarter), quarter), :]

    def finish_mixed():
        drain(p_in.at[pl.ds(0, TP - 1)], one_recv.at[6])
        projected = jnp.zeros((quarter, p_in.shape[2]), f32)
        for i in range(TP):
            projected = projected + p_in[i].astype(f32)
        mixed_out[...] = rms(projected, out_gain[...]).astype(bf16)

    take(0)
    take(1)
    relay(X, 0, x_recv, 4)
    take(2)
    relay(X, 1, x_recv, 4)
    take(3)
    relay(X, 2, x_recv, 4)
    load_g.wait()
    load_u.wait()
    hidden(0)
    take(4)
    relay(X, 3, x_recv, 4)
    take(5)
    relay(X, 4, x_recv, 4)
    hidden(1)
    hidden_relay(0)
    take(6)
    relay(X, 5, x_recv, 4)
    take(7)
    relay(X, 6, x_recv, 4)
    expand()
    hidden(2)
    relay(X, 7, x_recv, 4)
    hidden_relay(1)
    load_d.wait()
    drain(wd.at[pl.ds(0, TP - 1)], one_recv.at[0])
    down(0)
    head(0)
    hidden(3)
    hidden_relay(2)
    down(1)
    head(1)
    hidden_relay(3)
    down(2)
    head(2)
    down(3)
    head(3)
    give_back()
    project()
    finish_mixed()

    drain(R.at[pl.ds(0, slots - cell)], one_recv.at[3])
    total = jnp.dot(w_hi[...], R[...], preferred_element_type=f32)
    total = total + jnp.dot(w_lo[...], R[...], preferred_element_type=f32)
    m_send[...] = total.astype(bf16)
    for step in range(1, TP):
        peer = lax.rem(t + step, TP)
        place = pl.ds(pl.multiple_of(peer * quarter, quarter), quarter)
        send(m_send.at[place], m_recv.at[t], send_sem.at[12], one_recv.at[7], e, peer)
    m_recv[t] = m_send[pl.ds(pl.multiple_of(t * quarter, quarter), quarter), :]
    drain(m_recv.at[pl.ds(0, TP - 1)], one_recv.at[7])
    for i in range(TP):
        moe_out[:, i * width : (i + 1) * width] = m_recv[i]

    drain(outg.at[pl.ds(0, slots - cell)], send_sem.at[0])
    drain(wd.at[pl.ds(0, TP - 1)], send_sem.at[1])
    drain(Q.at[pl.ds(0, J - 1)], send_sem.at[2])
    drain(KV.at[pl.ds(0, NZ - 1)], send_sem.at[3])
    drain(X.at[pl.ds(0, 2)], send_sem.at[4])
    drain(X.at[0], send_sem.at[5])
    drain(H.at[pl.ds(0, 2)], send_sem.at[6])
    drain(H.at[0], send_sem.at[7])
    drain(Dn.at[pl.ds(0, slots - cell)], send_sem.at[8])
    drain(o_in.at[pl.ds(0, J - 1)], send_sem.at[9])
    drain(t_in.at[pl.ds(0, J - 1)], send_sem.at[10])
    drain(p_in.at[pl.ds(0, TP - 1)], send_sem.at[11])
    drain(m_recv.at[pl.ds(0, TP - 1)], send_sem.at[12])


def turn_tables(devices, rows):
    inverse = rope_base ** (-np.arange(0, ROPE, 2) / ROPE)
    inverse = np.tile(inverse, 4)[None, :]
    base = np.arange(devices)[:, None] * rows * inverse
    row = np.arange(rows)[:, None] * inverse
    return (
        np.concatenate([np.cos(base), np.sin(base)], axis=1).astype(np.float32),
        np.concatenate([np.cos(row), np.sin(row)], axis=1).astype(np.float32),
    )


def solution(mesh):
    EP, TP = mesh.shape["ep"], mesh.shape["tp"]
    J = 8
    NZ = EP // J
    placed = (
        P("ep", None),
        P(),
        P(None, "tp"),
        P(),
        P(),
        P(),
        P(None, "tp"),
        P(None, "tp"),
        P("tp", None),
        P(),
        P("ep", None),
        P(),
        P("ep", None, "tp"),
        P("ep", None, "tp"),
        P("ep", "tp", None),
        P("ep", None),
        P("ep", None),
    )

    def local(
        mix_in,
        mix_gain,
        query_weight,
        latent_weight,
        rotary_weight,
        latent_gain,
        key_weight,
        value_weight,
        output_weight,
        out_gain,
        ffn_in,
        ffn_gain,
        gate_weight,
        up_weight,
        down_weight,
        routes,
        route_scores,
    ):
        rows, D = mix_in.shape
        width = D // TP
        cell = MOST * (rows // QB)
        slots = EP * cell
        unit = gate_weight.shape[2]
        quarter = rows // TP
        base_turn, row_turn = turn_tables(EP, rows)
        hbm = pl.BlockSpec(memory_space=pl.ANY)
        vmem = pl.BlockSpec(memory_space=pltpu.VMEM)
        V = lambda *shape: pltpu.VMEM(shape, bf16)
        F = lambda *shape: pltpu.VMEM(shape, f32)
        S = pltpu.SemaphoreType.DMA

        def body(*refs):
            kernel(NZ, J, TP, *refs)

        out = jax.ShapeDtypeStruct((quarter, D), bf16)
        return pl.pallas_call(
            body,
            name="layer",
            out_shape=(out, out),
            in_specs=[
                hbm, vmem, hbm, hbm, hbm, vmem, hbm, hbm, hbm, vmem,
                hbm, vmem, hbm, hbm, hbm, vmem, vmem, vmem, vmem,
            ],
            out_specs=(vmem, vmem),
            scratch_shapes=[
                V(rows, D),
                V(rows, D),
                V(D, query_weight.shape[1]),
                V(D, latent_weight.shape[1]),
                V(D, ROPE),
                V(*key_weight.shape),
                V(*value_weight.shape),
                V(*output_weight.shape),
                V(D, unit),
                V(D, unit),
                V(TP, unit, width),
                V(slots, width),
                V(TP, slots, width),
                V(TP, slots, unit),
                V(slots, width),
                V(slots, width),
                V(rows, slots),
                V(rows, slots),
                V(rows, slots),
                V(rows, width),
                V(TP, quarter, width),
                V(J, rows, 768),
                V(NZ, rows, 640),
                V(rows, 768),
                V(rows, 640),
                V(4, NZ * rows, 256),
                V(4, NZ * rows, 256),
                V(J * rows, 512),
                F(J * rows, 128),
                V(J, rows, 512),
                F(J, rows, 128),
                V(rows, D),
                V(TP, quarter, D),
                S((11,)),
                S((8,)),
                S((3, 8)),
                S((3, 8)),
                S((8,)),
                S((13,)),
            ],
            compiler_params=pltpu.CompilerParams(
                collective_id=0, has_side_effects=True, vmem_limit_bytes=62 * 1024 * 1024
            ),
        )(
            mix_in,
            mix_gain[None, :],
            query_weight,
            latent_weight,
            rotary_weight,
            latent_gain[None, :],
            key_weight,
            value_weight,
            output_weight,
            out_gain[None, :],
            ffn_in,
            ffn_gain[None, :],
            gate_weight,
            up_weight,
            down_weight,
            routes,
            route_scores,
            base_turn,
            row_turn,
        )

    return jax.shard_map(
        local,
        mesh=mesh,
        in_specs=placed,
        out_specs=(P(("ep", "tp"), None), P(("ep", "tp"), None)),
        check_vma=False,
    )
```

profile of v0, /device:TPU:1, one launch (start us, length us, event | category | flops | bytes accessed | tf_op | source)
XLA Modules:
  0.0 132.0 jit_solution(6012916461927710177)
XLA Ops:
  0.6 1.4 %copy.22.refs_15_ = s32[128,4]{1,0:T(8,128)} copy(s32[128,4]{0,1:T(4,128)} %param.34) | data formatting | bytes 4096 | tf_op args[15]
  2.0 1.4 %copy.23.refs_16_ = f32[128,4]{1,0:T(8,128)} copy(f32[128,4]{0,1:T(4,128)} %param.35) | data formatting | bytes 4096 | tf_op args[16]
  3.5 1.9 %copy.21.refs_4_ = bf16[2048,64]{1,0:T(8,128)(2,1)} copy(bf16[2048,64]{0,1:T(8,128)(2,1)} %param.23) | data formatting | bytes 524288 | tf_op args[4]
  5.4 123.5 %layer.1 = (bf16[32,2048]{1,0:T(8,128)(2,1)}, bf16[32,2048]{1,0:T(8,128)(2,1)}) custom-call(bf16[128,2048]{1,0:T(8,128)(2,1)} %refs_0_.1, f32[1,2048]{1,0:T(1,128)} %bitcast.4, bf16[2048,768]{1,0:T(8,128)(2,1)} %refs_2_.1, bf16[2048,512]{1,0:T(8,128)(2,1)} %refs_3_.1, bf16[2048,64]{1,0:T(8,128)(2,1)} %copy.21.refs_4_, f32[1,512]{1,0:T(1,128)} %bitcast.7, ...), custom_call_target="tpu_custom_call" | custom-call | tf_op jit(solution)/shard_map/layer/pallas_call | solution.py:605
  128.9 1.6 %copy.26 = bf16[32,2048]{1,0:T(8,128)(2,1)} copy(bf16[32,2048]{1,0:T(8,128)(2,1)} %get-tuple-element.4) | data formatting | bytes 262144
  130.5 1.6 %copy.27 = bf16[32,2048]{1,0:T(8,128)(2,1)} copy(bf16[32,2048]{1,0:T(8,128)(2,1)} %get-tuple-element.5) | data formatting | bytes 262144
where the time goes:
time: 132 us
  Pallas kernels  123 us (93%)
  local copies, waits for them, and re-layouts  7.91 us (6%)
    pallas_call x1, Pallas kernels, local(): pl.pallas_call(body, name='layer', out_shape=(out, out), in_specs=[hbm, v...  123 us
    unnamed x5, local copies, waits for them, and re-layouts  7.91 us

commit v1 on v0

--- a/solution.py
+++ b/solution.py
@@ -21,7 +21,7 @@
 bf16 = jnp.bfloat16
 f32 = jnp.float32
 
-ORDER = (0, 1, 7, 2, 6, 3, 5, 4)
+ORDER = (0, 1, 4, 3, 5, 6, 2, 7)
 
 
 def iota(shape, dim):
@@ -34,7 +34,8 @@
 
 
 def drain(view, sem):
-    pltpu.make_async_copy(view, view, sem).wait()
+    with jax.named_scope("wait"):
+        pltpu.make_async_copy(view, view, sem).wait()
 
 
 def kernel(
@@ -74,6 +75,7 @@
     uw,
     wd,
     outg,
+    near,
     X,
     H,
     Dn,
@@ -86,11 +88,11 @@
     Q,
     KV,
     q_out,
-    kv_out,
     Kc,
     Vc,
     o_out,
     t_out,
+    t_row,
     o_in,
     t_in,
     p_out,
@@ -99,6 +101,7 @@
     disp_recv,
     x_recv,
     h_recv,
+    kv_recv,
     one_recv,
     send_sem,
 ):
@@ -145,11 +148,12 @@
 
     barrier = pltpu.get_barrier_semaphore()
 
-    @pl.loop(1, E)
-    def _(step):
-        pl.semaphore_signal(
-            barrier, inc=1, device_id=(lax.rem(e + step, E), t), device_id_type=MESH
-        )
+    for dz in (4, 3, 5, 2, 6, 1, 7, 0):
+
+        @pl.loop(1 if dz == 0 else 0, J)
+        def _(step, dz=dz):
+            peer = lax.rem(z + dz, NZ) * J + lax.rem(j + step, J)
+            pl.semaphore_signal(barrier, inc=1, device_id=(peer, t), device_id_type=MESH)
 
     for step in range(1, TP):
         pl.semaphore_signal(
@@ -158,51 +162,59 @@
 
     slots = outg.shape[0]
     blocks = rows // QB
-    slot = iota((1, slots), 1)
+    slot = iota((slots, 1), 0)
     slot_expert = slot // cell
     slot_block = (slot // MOST) % blocks
     slot_rank = (slot % MOST).astype(f32)
-    row_block = iota((rows, 1), 0) // QB
+    row_block = iota((1, rows), 1) // QB
     route = routes[...]
-    choose = route.shape[1]
-    named = jnp.zeros((rows, slots), f32)
+    choose = route.shape[0]
+    named = jnp.zeros((slots, rows), f32)
     for k in range(choose):
-        named = named + jnp.where(route[:, k : k + 1] == slot_expert, 1.0, 0.0)
-    low_r = iota((rows, rows), 0)
-    low_c = iota((rows, rows), 1)
-    lower = jnp.where((low_c < low_r) & (low_c // QB == low_r // QB), 1.0, 0.0).astype(bf16)
-    rank = jnp.dot(lower, named.astype(bf16), preferred_element_type=f32)
+        named = named + jnp.where(route[k : k + 1, :] == slot_expert, 1.0, 0.0)
+    up_r = iota((rows, rows), 0)
+    up_c = iota((rows, rows), 1)
+    upper = jnp.where((up_r < up_c) & (up_c // QB == up_r // QB), 1.0, 0.0).astype(bf16)
+    rank = jnp.dot(named.astype(bf16), upper, preferred_element_type=f32)
     picked = jnp.where((rank == slot_rank) & (row_block == slot_block), named, 0.0)
     sel[...] = picked.astype(bf16)
 
     load_ffn.wait()
-    x = ffn_v[...].astype(f32)
-    inverse = lax.rsqrt(jnp.mean(x * x, axis=-1, keepdims=True) + norm_eps)
+    ffn_v[...] = rms(ffn_v[...].astype(f32), ffn_gain[...]).astype(bf16)
     columns = pl.ds(pl.multiple_of(t * width, 128), width)
-    normed_part = (ffn_v[:, columns].astype(f32) * inverse * ffn_gain[:, columns]).astype(bf16)
-    outg[...] = lax.dot_general(
-        sel[...], normed_part, (((0,), (0,)), ((), ())), preferred_element_type=f32
-    ).astype(bf16)
-
-    pl.semaphore_wait(barrier, E - 1 + TP - 1)
-
-    my_rows = pl.ds(pl.multiple_of(e * cell, cell), cell)
-    for number, dz in enumerate(ORDER):
-        target_z = lax.rem(z + NZ - dz, NZ)
-
-        @pl.loop(1 if dz == 0 else 0, J)
-        def _(step, number=number, target_z=target_z):
-            target = target_z * J + lax.rem(j + step, J)
-            send(
-                outg.at[pl.ds(pl.multiple_of(target * cell, cell), cell)],
-                X.at[t, my_rows],
-                send_sem.at[0],
-                disp_recv.at[number],
-                target,
-                t,
-            )
-
-    X[t, my_rows] = outg[my_rows, :]
+    outg[...] = jnp.dot(sel[...], ffn_v[:, columns], preferred_element_type=f32).astype(bf16)
+    own_z = pl.ds(pl.multiple_of(z * unit, unit), unit)
+    for part in range(TP):
+        near[part] = jnp.dot(
+            sel[own_z, :], ffn_v[:, part * width : (part + 1) * width], preferred_element_type=f32
+        ).astype(bf16)
+
+    base = base_turn[pl.ds(e, 1), :]
+    base_cos, base_sin = base[:, :128], base[:, 128:]
+    row_cos, row_sin = row_turn[:, :128], row_turn[:, 128:]
+    cosine = base_cos * row_cos - base_sin * row_sin
+    sine = base_sin * row_cos + base_cos * row_sin
+    lane = iota((rows, 128), 1)
+    first_half = lane % ROPE < ROPE // 2
+    sine = jnp.where(first_half, -sine, sine)
+
+    def turned(v):
+        partner = jnp.where(first_half, pltpu.roll(v, 96, 1), pltpu.roll(v, 32, 1))
+        return v * cosine + partner * sine
+
+    load_mix.wait()
+    mix_v[...] = rms(mix_v[...].astype(f32), mix_gain[...]).astype(bf16)
+    load_l.wait()
+    latent = jnp.dot(mix_v[...], lw[...], preferred_element_type=f32)
+    KV[z, :, 0:512] = rms(latent, latent_gain[...]).astype(bf16)
+    load_r.wait()
+    rotary = lax.dot_general(
+        mix_v[...], rw[...], (((1,), (1,)), ((), ())), preferred_element_type=f32
+    )
+    KV[z, :, 512:640] = turned(jnp.concatenate([rotary, rotary], axis=1)).astype(bf16)
+
+    with jax.named_scope("barrier"):
+        pl.semaphore_wait(barrier, E - 1 + TP - 1)
 
     for step in range(1, TP):
         peer = lax.rem(t + step, TP)
@@ -215,23 +227,64 @@
             peer,
         )
 
-    load_mix.wait()
-    normed = rms(mix_v[...].astype(f32), mix_gain[...]).astype(bf16)
+    my_rows = pl.ds(pl.multiple_of(e * cell, cell), cell)
+
+    @pl.loop(1, J)
+    def _(step):
+        to = lax.rem(j + step, J)
+        send(
+            near.at[:, pl.ds(pl.multiple_of(to * cell, cell), cell)],
+            X.at[:, my_rows],
+            send_sem.at[0],
+            disp_recv.at[0],
+            z * J + to,
+            t,
+        )
+
+    for part in range(TP):
+        X[part, my_rows] = near[part, pl.ds(pl.multiple_of(j * cell, cell), cell)]
+
+    def dispatch(number):
+        target_z = lax.rem(z + NZ - ORDER[number], NZ)
+
+        @pl.loop(0, J)
+        def _(step):
+            target = target_z * J + lax.rem(j + step, J)
+            send(
+                outg.at[pl.ds(pl.multiple_of(target * cell, cell), cell)],
+                X.at[t, my_rows],
+                send_sem.at[13],
+                disp_recv.at[number],
+                target,
+                t,
+            )
+
+    up_z, down_z = lax.rem(z + 1, NZ), lax.rem(z + NZ - 1, NZ)
+    half = rows // 2
+
+    def pass_on(hop):
+        if hop > 0:
+            at_up, at_down = lax.rem(z + NZ - hop, NZ), lax.rem(z + hop, NZ)
+            drain(KV.at[at_up], kv_recv.at[0, hop - 1])
+            drain(KV.at[at_down], kv_recv.at[1, hop - 1])
+        else:
+            at_up = at_down = z
+        upward, downward = KV.at[at_up], KV.at[at_down]
+        if 2 * (hop + 1) == NZ:
+            upward, downward = KV.at[at_up, pl.ds(0, half)], KV.at[at_down, pl.ds(half, half)]
+        send(upward, upward, send_sem.at[3], kv_recv.at[0, hop], up_z * J + j, t)
+        send(downward, downward, send_sem.at[3], kv_recv.at[1, hop], down_z * J + j, t)
+
+    def latents_here():
+        across = lax.rem(z + NZ // 2, NZ)
+        drain(KV.at[across, pl.ds(0, half)], kv_recv.at[0, NZ // 2 - 1])
+        drain(KV.at[across, pl.ds(half, half)], kv_recv.at[1, NZ // 2 - 1])
+
+    pass_on(0)
+    dispatch(1)
+
     load_q.wait()
-    queries = jnp.dot(normed, qw[...], preferred_element_type=f32)
-    base = base_turn[pl.ds(e, 1), :]
-    base_cos, base_sin = base[:, :128], base[:, 128:]
-    row_cos, row_sin = row_turn[:, :128], row_turn[:, 128:]
-    cosine = base_cos * row_cos - base_sin * row_sin
-    sine = base_sin * row_cos + base_cos * row_sin
-    lane = iota((rows, 128), 1)
-    first_half = lane % ROPE < ROPE // 2
-    sine = jnp.where(first_half, -sine, sine)
-
-    def turned(v):
-        partner = jnp.where(first_half, pltpu.roll(v, 96, 1), pltpu.roll(v, 32, 1))
-        return v * cosine + partner * sine
-
+    queries = jnp.dot(mix_v[...], qw[...], preferred_element_type=f32)
     low_lanes = lane < 64
     A = [queries[:, 128 * i : 128 * (i + 1)] for i in range(6)]
     q_out[:, 0:128] = A[0].astype(bf16)
@@ -240,42 +293,25 @@
     q_out[:, 384:512] = pltpu.roll(jnp.where(low_lanes, A[5], A[4]), 64, 1).astype(bf16)
     q_out[:, 512:640] = turned(jnp.where(low_lanes, A[1], A[2])).astype(bf16)
     q_out[:, 640:768] = turned(jnp.where(low_lanes, A[4], A[5])).astype(bf16)
-
-    load_l.wait()
-    latent = jnp.dot(normed, lw[...], preferred_element_type=f32)
-    kv_out[:, 0:512] = rms(latent, latent_gain[...]).astype(bf16)
-    load_r.wait()
-    rotary = jnp.dot(normed, rw[...], preferred_element_type=f32)
-    kv_out[:, 512:640] = turned(jnp.concatenate([rotary, rotary], axis=1)).astype(bf16)
-
-    for step in range(1, J):
-        send(
-            q_out,
-            Q.at[j],
-            send_sem.at[2],
-            one_recv.at[1],
-            z * J + lax.rem(j + step, J),
-            t,
-        )
-    for step in (1, 7, 2, 6, 3, 5, 4):
-        send(
-            kv_out,
-            KV.at[z],
-            send_sem.at[3],
-            one_recv.at[2],
-            lax.rem(z + step, NZ) * J + j,
-            t,
-        )
     Q[j] = q_out[...]
-    KV[z] = kv_out[...]
+    mate = j + 1 - 2 * lax.rem(j, 2)
+    for step in range(2, J, 2):
+        send(Q.at[j], Q.at[j], send_sem.at[2], one_recv.at[1], z * J + lax.rem(j + step, J), t)
+    send(Q.at[j], Q.at[j], send_sem.at[14], one_recv.at[8], z * J + mate, t)
+
+    def share_queries():
+        drain(Q.at[pl.ds(0, J // 2 - 1)], one_recv.at[1])
+        for step in range(2, J, 2):
+            from_j = lax.rem(j + step, J)
+            send(Q.at[from_j], Q.at[from_j], send_sem.at[14], one_recv.at[8], z * J + mate, t)
 
     score = route_scores[...]
-    grown = jnp.exp(score - jnp.max(score, axis=-1, keepdims=True))
-    share = grown / jnp.sum(grown, axis=-1, keepdims=True)
-    gates = jnp.zeros((rows, slots), f32)
+    grown = jnp.exp(score - jnp.max(score, axis=0, keepdims=True))
+    share = grown / jnp.sum(grown, axis=0, keepdims=True)
+    gates = jnp.zeros((slots, rows), f32)
     for k in range(choose):
-        gates = gates + jnp.where(route[:, k : k + 1] == slot_expert, share[:, k : k + 1], 0.0)
-    gates = gates * sel[...].astype(f32)
+        gates = gates + jnp.where(route[k : k + 1, :] == slot_expert, share[k : k + 1, :], 0.0)
+    gates = jnp.transpose(gates * sel[...].astype(f32))
     gates_hi = gates.astype(bf16)
     w_hi[...] = gates_hi
     w_lo[...] = (gates - gates_hi.astype(f32)).astype(bf16)
@@ -317,16 +353,17 @@
         drain(buf.at[across, unit_rows(number)], sems.at[2, number])
 
     def take(number):
-        if ORDER[number] == 0:
-            drain(X.at[t, pl.ds(0, unit - cell)], disp_recv.at[number])
+        if number == 0:
+            drain(X.at[:, pl.ds(0, unit - cell)], disp_recv.at[0])
         else:
             drain(X.at[t, pl.ds(0, unit)], disp_recv.at[number])
-        spread(X, number, x_recv, 4)
+            spread(X, number, x_recv, 4)
 
     def hidden(batch):
         pair = (2 * batch, 2 * batch + 1)
         for number in pair:
-            relayed(X, number, x_recv)
+            if number > 0:
+                relayed(X, number, x_recv)
         gate_part = jnp.zeros((2 * unit, gw.shape[1]), f32)
         up_part = jnp.zeros((2 * unit, gw.shape[1]), f32)
         for part in range(TP):
@@ -376,8 +413,8 @@
                 R[my_rows, :] = Dn[my_rows, :]
 
     def expand():
-        drain(Q.at[pl.ds(0, J - 1)], one_recv.at[1])
-        drain(KV.at[pl.ds(0, NZ - 1)], one_recv.at[2])
+        drain(Q.at[pl.ds(0, J // 2)], one_recv.at[8])
+        latents_here()
         load_k.wait()
         load_v.wait()
         lat = KV[...].reshape(NZ * rows, 640)
@@ -423,14 +460,17 @@
                 t_out[here, :] = jnp.where(lanes // 32 == h, sums, t_out[here, :])
 
     def give_back():
-        for step in range(1, J):
+        for i in range(J):
+            across = jnp.transpose(t_out[i * rows : (i + 1) * rows, :])
+            picks = [across[32 * h : 32 * h + 1, :] for h in range(4)]
+            t_row[i] = jnp.concatenate(picks + picks, axis=0)
+        for step in (4, 2, 6, 3, 5, 1, 7):
             target = lax.rem(j + step, J)
             place = pl.ds(pl.multiple_of(target * rows, rows), rows)
             send(o_out.at[place], o_in.at[j], send_sem.at[9], one_recv.at[4], z * J + target, t)
-            send(t_out.at[place], t_in.at[j], send_sem.at[10], one_recv.at[5], z * J + target, t)
-        place = pl.ds(pl.multiple_of(j * rows, rows), rows)
-        o_in[j] = o_out[place, :]
-        t_in[j] = t_out[place, :]
+            send(t_row.at[target], t_in.at[j], send_sem.at[10], one_recv.at[5], z * J + target, t)
+        o_in[j] = o_out[pl.ds(pl.multiple_of(j * rows, rows), rows), :]
+        t_in[j] = t_row[j]
 
     quarter = rows // TP
 
@@ -439,12 +479,13 @@
         drain(t_in.at[pl.ds(0, J - 1)], one_recv.at[5])
         load_o.wait()
         osum = jnp.zeros((rows, 4 * VD), f32)
-        tsum = jnp.zeros((rows, 128), f32)
+        tsum = jnp.zeros(t_in.shape[1:], f32)
         for i in range(J):
             osum = osum + o_in[i].astype(f32)
             tsum = tsum + t_in[i]
+        tsum = jnp.transpose(jnp.concatenate([tsum] * (128 // tsum.shape[0]), axis=0))
         heads = [
-            (osum[:, VD * h : VD * (h + 1)] / tsum[:, 32 * h : 32 * h + 1]).astype(bf16)
+            (osum[:, VD * h : VD * (h + 1)] / tsum[:, h : h + 1]).astype(bf16)
             for h in range(4)
         ]
         attended = jnp.concatenate(heads, axis=1)
@@ -462,48 +503,105 @@
             projected = projected + p_in[i].astype(f32)
         mixed_out[...] = rms(projected, out_gain[...]).astype(bf16)
 
-    take(0)
-    take(1)
-    relay(X, 0, x_recv, 4)
-    take(2)
-    relay(X, 1, x_recv, 4)
-    take(3)
-    relay(X, 2, x_recv, 4)
-    load_g.wait()
-    load_u.wait()
-    hidden(0)
-    take(4)
-    relay(X, 3, x_recv, 4)
-    take(5)
-    relay(X, 4, x_recv, 4)
-    hidden(1)
-    hidden_relay(0)
-    take(6)
-    relay(X, 5, x_recv, 4)
-    take(7)
-    relay(X, 6, x_recv, 4)
-    expand()
-    hidden(2)
-    relay(X, 7, x_recv, 4)
-    hidden_relay(1)
-    load_d.wait()
-    drain(wd.at[pl.ds(0, TP - 1)], one_recv.at[0])
-    down(0)
-    head(0)
-    hidden(3)
-    hidden_relay(2)
-    down(1)
-    head(1)
-    hidden_relay(3)
-    down(2)
-    head(2)
-    down(3)
-    head(3)
-    give_back()
-    project()
-    finish_mixed()
-
-    drain(R.at[pl.ds(0, slots - cell)], one_recv.at[3])
+    with jax.named_scope("s00_pass_on_1"):
+        pass_on(1)
+    with jax.named_scope("s01_dispatch_2"):
+        dispatch(2)
+    with jax.named_scope("s02_take_0"):
+        take(0)
+    with jax.named_scope("s03_take_1"):
+        take(1)
+    with jax.named_scope("s04_pass_on_2"):
+        pass_on(2)
+    with jax.named_scope("s05_dispatch_3"):
+        dispatch(3)
+    with jax.named_scope("s06_dispatch_4"):
+        dispatch(4)
+    with jax.named_scope("s07_share_queries_"):
+        share_queries()
+    with jax.named_scope("s08_relay_X_1"):
+        relay(X, 1, x_recv, 4)
+    with jax.named_scope("s09_take_2"):
+        take(2)
+    with jax.named_scope("s10_load_gu_"):
+        load_g.wait()
+        load_u.wait()
+    with jax.named_scope("s11_hidden_0"):
+        hidden(0)
+    with jax.named_scope("s12_pass_on_3"):
+        pass_on(3)
+    with jax.named_scope("s13_dispatch_5"):
+        dispatch(5)
+    with jax.named_scope("s14_dispatch_6"):
+        dispatch(6)
+    with jax.named_scope("s15_dispatch_7"):
+        dispatch(7)
+    with jax.named_scope("s16_relay_X_2"):
+        relay(X, 2, x_recv, 4)
+    with jax.named_scope("s17_hidden_relay_0"):
+        hidden_relay(0)
+    with jax.named_scope("s18_take_3"):
+        take(3)
+    with jax.named_scope("s19_take_4"):
+        take(4)
+    with jax.named_scope("s20_relay_X_3"):
+        relay(X, 3, x_recv, 4)
+    with jax.named_scope("s21_expand_"):
+        expand()
+    with jax.named_scope("s22_relay_X_4"):
+        relay(X, 4, x_recv, 4)
+    with jax.named_scope("s23_hidden_1"):
+        hidden(1)
+    with jax.named_scope("s24_head_0"):
+        head(0)
+    with jax.named_scope("s25_take_5"):
+        take(5)
+    with jax.named_scope("s26_load_dd_"):
+        load_d.wait()
+        drain(wd.at[pl.ds(0, TP - 1)], one_recv.at[0])
+    with jax.named_scope("s27_down_0"):
+        down(0)
+    with jax.named_scope("s28_head_1"):
+        head(1)
+    with jax.named_scope("s29_take_6"):
+        take(6)
+    with jax.named_scope("s30_relay_X_5"):
+        relay(X, 5, x_recv, 4)
+    with jax.named_scope("s31_hidden_relay_1"):
+        hidden_relay(1)
+    with jax.named_scope("s32_head_2"):
+        head(2)
+    with jax.named_scope("s33_take_7"):
+        take(7)
+    with jax.named_scope("s34_relay_X_6"):
+        relay(X, 6, x_recv, 4)
+    with jax.named_scope("s35_hidden_2"):
+        hidden(2)
+    with jax.named_scope("s36_down_1"):
+        down(1)
+    with jax.named_scope("s37_head_3"):
+        head(3)
+    with jax.named_scope("s38_relay_X_7"):
+        relay(X, 7, x_recv, 4)
+    with jax.named_scope("s39_hidden_relay_2"):
+        hidden_relay(2)
+    with jax.named_scope("s40_give_back_"):
+        give_back()
+    with jax.named_scope("s41_hidden_3"):
+        hidden(3)
+    with jax.named_scope("s42_down_2"):
+        down(2)
+    with jax.named_scope("s43_hidden_relay_3"):
+        hidden_relay(3)
+    with jax.named_scope("s44_project_"):
+        project()
+    with jax.named_scope("s45_down_3"):
+        down(3)
+    with jax.named_scope("s46_finish_mixed_"):
+        finish_mixed()
+
+    with jax.named_scope("returns"):
+        drain(R.at[pl.ds(0, slots - cell)], one_recv.at[3])
     total = jnp.dot(w_hi[...], R[...], preferred_element_type=f32)
     total = total + jnp.dot(w_lo[...], R[...], preferred_element_type=f32)
     m_send[...] = total.astype(bf16)
@@ -512,16 +610,20 @@
         place = pl.ds(pl.multiple_of(peer * quarter, quarter), quarter)
         send(m_send.at[place], m_recv.at[t], send_sem.at[12], one_recv.at[7], e, peer)
     m_recv[t] = m_send[pl.ds(pl.multiple_of(t * quarter, quarter), quarter), :]
-    drain(m_recv.at[pl.ds(0, TP - 1)], one_recv.at[7])
+    with jax.named_scope("last"):
+        drain(m_recv.at[pl.ds(0, TP - 1)], one_recv.at[7])
     for i in range(TP):
         moe_out[:, i * width : (i + 1) * width] = m_recv[i]
 
-    drain(outg.at[pl.ds(0, slots - cell)], send_sem.at[0])
+    most = slots - unit
+    drain(X.at[:, pl.ds(0, unit - cell)], send_sem.at[0])
+    drain(outg.at[pl.ds(0, most)], send_sem.at[13])
     drain(wd.at[pl.ds(0, TP - 1)], send_sem.at[1])
-    drain(Q.at[pl.ds(0, J - 1)], send_sem.at[2])
+    drain(Q.at[pl.ds(0, J // 2 - 1)], send_sem.at[2])
+    drain(Q.at[pl.ds(0, J // 2)], send_sem.at[14])
     drain(KV.at[pl.ds(0, NZ - 1)], send_sem.at[3])
-    drain(X.at[pl.ds(0, 2)], send_sem.at[4])
-    drain(X.at[0], send_sem.at[5])
+    drain(X.at[pl.ds(0, 2), pl.ds(0, most)], send_sem.at[4])
+    drain(X.at[0, pl.ds(0, most)], send_sem.at[5])
     drain(H.at[pl.ds(0, 2)], send_sem.at[6])
     drain(H.at[0], send_sem.at[7])
     drain(Dn.at[pl.ds(0, slots - cell)], send_sem.at[8])
@@ -616,7 +718,7 @@
                 V(rows, D),
                 V(D, query_weight.shape[1]),
                 V(D, latent_weight.shape[1]),
-                V(D, ROPE),
+                V(ROPE, D),
                 V(*key_weight.shape),
                 V(*value_weight.shape),
                 V(*output_weight.shape),
@@ -624,11 +726,12 @@
                 V(D, unit),
                 V(TP, unit, width),
                 V(slots, width),
+                V(TP, J * cell, width),
                 V(TP, slots, width),
                 V(TP, slots, unit),
                 V(slots, width),
                 V(slots, width),
-                V(rows, slots),
+                V(slots, rows),
                 V(rows, slots),
                 V(rows, slots),
                 V(rows, width),
@@ -636,21 +739,22 @@
                 V(J, rows, 768),
                 V(NZ, rows, 640),
                 V(rows, 768),
-                V(rows, 640),
                 V(4, NZ * rows, 256),
                 V(4, NZ * rows, 256),
                 V(J * rows, 512),
                 F(J * rows, 128),
+                F(J, 8, rows),
                 V(J, rows, 512),
-                F(J, rows, 128),
+                F(J, 8, rows),
                 V(rows, D),
                 V(TP, quarter, D),
                 S((11,)),
                 S((8,)),
                 S((3, 8)),
                 S((3, 8)),
-                S((8,)),
-                S((13,)),
+                S((2, NZ // 2)),
+                S((9,)),
+                S((15,)),
             ],
             compiler_params=pltpu.CompilerParams(
                 collective_id=0, has_side_effects=True, vmem_limit_bytes=62 * 1024 * 1024
@@ -660,7 +764,7 @@
             mix_gain[None, :],
             query_weight,
             latent_weight,
-            rotary_weight,
+            rotary_weight.T,
             latent_gain[None, :],
             key_weight,
             value_weight,
@@ -671,8 +775,8 @@
             gate_weight,
             up_weight,
             down_weight,
-            routes,
-            route_scores,
+            routes.T,
+            route_scores.T,
             base_turn,
             row_turn,
         )

time: 132 us -> 112 us (0.85)
  Pallas kernels: 123 us -> 107 us
  local copies, waits for them, and re-layouts: 7.91 us -> 3.14 us
    pallas_call x1, Pallas kernels: 123 us -> 107 us  [local(): pl.pallas_call(body, name='layer', out_shape=(out, out), in_specs=[hbm, v...]
    unnamed x5 -> x2, local copies, waits for them, and re-layouts: 7.91 us -> 3.14 us
where the time goes in v1:
time: 112 us; the launch traced here: 111 us
  Pallas kernels  107 us (96%)
  local copies, waits for them, and re-layouts  3.14 us (3%)
    pallas_call x1, Pallas kernels, local(): pl.pallas_call(body, name='layer', out_shape=(out, out), in_specs=[hbm, v...  107 us
    unnamed x2, local copies, waits for them, and re-layouts  3.14 us

profile of v1, /device:TPU:1, one launch (start us, length us, event | category | flops | bytes accessed | tf_op | source)
XLA Modules:
  0.0 110.8 jit_solution(11762265637212584251)
XLA Ops:
  0.6 107.0 %layer.1 = (bf16[32,2048]{1,0:T(8,128)(2,1)}, bf16[32,2048]{1,0:T(8,128)(2,1)}) custom-call(bf16[128,2048]{1,0:T(8,128)(2,1)} %refs_0_.1, f32[1,2048]{1,0:T(1,128)} %bitcast.8, bf16[2048,768]{1,0:T(8,128)(2,1)} %refs_2_.1, bf16[2048,512]{1,0:T(8,128)(2,1)} %refs_3_.1, bf16[64,2048]{1,0:T(8,128)(2,1)} %bitcast.7, f32[1,512]{1,0:T(1,128)} %bitcast.11, ...), custom_call_target="tpu_custom_call" | custom-call | tf_op jit(solution)/shard_map/layer/pallas_call | solution.py:707
  107.6 1.6 %copy.23 = bf16[32,2048]{1,0:T(8,128)(2,1)} copy(bf16[32,2048]{1,0:T(8,128)(2,1)} %get-tuple-element.4) | data formatting | bytes 262144
  109.2 1.6 %copy.24 = bf16[32,2048]{1,0:T(8,128)(2,1)} copy(bf16[32,2048]{1,0:T(8,128)(2,1)} %get-tuple-element.5) | data formatting | bytes 262144

commit v2 on v1

--- a/solution.py
+++ b/solution.py
@@ -21,7 +21,7 @@
 bf16 = jnp.bfloat16
 f32 = jnp.float32
 
-ORDER = (0, 1, 4, 3, 5, 6, 2, 7)
+ORDER = (0, 4, 3, 5, 2, 6, 1, 7)
 
 
 def iota(shape, dim):
@@ -202,17 +202,6 @@
         partner = jnp.where(first_half, pltpu.roll(v, 96, 1), pltpu.roll(v, 32, 1))
         return v * cosine + partner * sine
 
-    load_mix.wait()
-    mix_v[...] = rms(mix_v[...].astype(f32), mix_gain[...]).astype(bf16)
-    load_l.wait()
-    latent = jnp.dot(mix_v[...], lw[...], preferred_element_type=f32)
-    KV[z, :, 0:512] = rms(latent, latent_gain[...]).astype(bf16)
-    load_r.wait()
-    rotary = lax.dot_general(
-        mix_v[...], rw[...], (((1,), (1,)), ((), ())), preferred_element_type=f32
-    )
-    KV[z, :, 512:640] = turned(jnp.concatenate([rotary, rotary], axis=1)).astype(bf16)
-
     with jax.named_scope("barrier"):
         pl.semaphore_wait(barrier, E - 1 + TP - 1)
 
@@ -280,8 +269,20 @@
         drain(KV.at[across, pl.ds(0, half)], kv_recv.at[0, NZ // 2 - 1])
         drain(KV.at[across, pl.ds(half, half)], kv_recv.at[1, NZ // 2 - 1])
 
+    dispatch(1)
+    load_mix.wait()
+    mix_v[...] = rms(mix_v[...].astype(f32), mix_gain[...]).astype(bf16)
+    load_l.wait()
+    latent = jnp.dot(mix_v[...], lw[...], preferred_element_type=f32)
+    KV[z, :, 0:512] = rms(latent, latent_gain[...]).astype(bf16)
+    load_r.wait()
+    rotary = lax.dot_general(
+        mix_v[...], rw[...], (((1,), (1,)), ((), ())), preferred_element_type=f32
+    )
+    KV[z, :, 512:640] = turned(jnp.concatenate([rotary, rotary], axis=1)).astype(bf16)
+
     pass_on(0)
-    dispatch(1)
+    dispatch(2)
 
     load_q.wait()
     queries = jnp.dot(mix_v[...], qw[...], preferred_element_type=f32)
@@ -451,7 +452,7 @@
             weights = jnp.where(key_place <= query_place, jnp.exp(scores * scale), 0.0).astype(bf16)
             both_out = jnp.dot(weights, Vc[h], preferred_element_type=f32)
             here = pl.ds(pl.multiple_of(chunk * span, span), span)
-            o_out[here, 128 * h : 128 * (h + 1)] = both_out[:, :128].astype(bf16)
+            o_out[h, here, :] = both_out[:, :128].astype(bf16)
             sums = both_out[:, 128:]
             if h == 0:
                 t_out[here, :] = sums
@@ -459,35 +460,41 @@
                 lanes = iota((span, 128), 1)
                 t_out[here, :] = jnp.where(lanes // 32 == h, sums, t_out[here, :])
 
-    def give_back():
+    back_order = (4, 2, 6, 3, 5, 1, 7)
+
+    def give_back(h):
+        for step in back_order:
+            target = lax.rem(j + step, J)
+            place = pl.ds(pl.multiple_of(target * rows, rows), rows)
+            send(o_out.at[h, place], o_in.at[h, j], send_sem.at[9], one_recv.at[4], z * J + target, t)
+        o_in[h, j] = o_out[h, pl.ds(pl.multiple_of(j * rows, rows), rows), :]
+
+    def give_totals():
         for i in range(J):
             across = jnp.transpose(t_out[i * rows : (i + 1) * rows, :])
             picks = [across[32 * h : 32 * h + 1, :] for h in range(4)]
             t_row[i] = jnp.concatenate(picks + picks, axis=0)
-        for step in (4, 2, 6, 3, 5, 1, 7):
+        for step in back_order:
             target = lax.rem(j + step, J)
-            place = pl.ds(pl.multiple_of(target * rows, rows), rows)
-            send(o_out.at[place], o_in.at[j], send_sem.at[9], one_recv.at[4], z * J + target, t)
             send(t_row.at[target], t_in.at[j], send_sem.at[10], one_recv.at[5], z * J + target, t)
-        o_in[j] = o_out[pl.ds(pl.multiple_of(j * rows, rows), rows), :]
         t_in[j] = t_row[j]
 
     quarter = rows // TP
 
     def project():
-        drain(o_in.at[pl.ds(0, J - 1)], one_recv.at[4])
+        drain(o_in.at[:, pl.ds(0, J - 1)], one_recv.at[4])
         drain(t_in.at[pl.ds(0, J - 1)], one_recv.at[5])
         load_o.wait()
-        osum = jnp.zeros((rows, 4 * VD), f32)
         tsum = jnp.zeros(t_in.shape[1:], f32)
         for i in range(J):
-            osum = osum + o_in[i].astype(f32)
             tsum = tsum + t_in[i]
         tsum = jnp.transpose(jnp.concatenate([tsum] * (128 // tsum.shape[0]), axis=0))
-        heads = [
-            (osum[:, VD * h : VD * (h + 1)] / tsum[:, h : h + 1]).astype(bf16)
-            for h in range(4)
-        ]
+        heads = []
+        for h in range(4):
+            osum = jnp.zeros((rows, VD), f32)
+            for i in range(J):
+                osum = osum + o_in[h, i].astype(f32)
+            heads.append((osum / tsum[:, h : h + 1]).astype(bf16))
         attended = jnp.concatenate(heads, axis=1)
         p_out[...] = jnp.dot(attended, ow[...], preferred_element_type=f32).astype(bf16)
         for step in range(1, TP):
@@ -503,101 +510,107 @@
             projected = projected + p_in[i].astype(f32)
         mixed_out[...] = rms(projected, out_gain[...]).astype(bf16)
 
-    with jax.named_scope("s00_pass_on_1"):
+    with jax.named_scope("s00_dispatch_7"):
+        dispatch(7)
+    with jax.named_scope("s01_dispatch_3"):
+        dispatch(3)
+    with jax.named_scope("s02_dispatch_4"):
+        dispatch(4)
+    with jax.named_scope("s03_pass_on_1"):
         pass_on(1)
-    with jax.named_scope("s01_dispatch_2"):
-        dispatch(2)
-    with jax.named_scope("s02_take_0"):
+    with jax.named_scope("s04_take_1"):
+        take(1)
+    with jax.named_scope("s05_relay_X_1"):
+        relay(X, 1, x_recv, 4)
+    with jax.named_scope("s06_take_7"):
+        take(7)
+    with jax.named_scope("s07_dispatch_6"):
+        dispatch(6)
+    with jax.named_scope("s08_dispatch_5"):
+        dispatch(5)
+    with jax.named_scope("s09_take_0"):
         take(0)
-    with jax.named_scope("s03_take_1"):
-        take(1)
-    with jax.named_scope("s04_pass_on_2"):
+    with jax.named_scope("s10_take_2"):
+        take(2)
+    with jax.named_scope("s11_take_3"):
+        take(3)
+    with jax.named_scope("s12_pass_on_2"):
         pass_on(2)
-    with jax.named_scope("s05_dispatch_3"):
-        dispatch(3)
-    with jax.named_scope("s06_dispatch_4"):
-        dispatch(4)
-    with jax.named_scope("s07_share_queries_"):
-        share_queries()
-    with jax.named_scope("s08_relay_X_1"):
-        relay(X, 1, x_recv, 4)
-    with jax.named_scope("s09_take_2"):
-        take(2)
-    with jax.named_scope("s10_load_gu_"):
+    with jax.named_scope("s13_load_gu_"):
         load_g.wait()
         load_u.wait()
-    with jax.named_scope("s11_hidden_0"):
+    with jax.named_scope("s14_hidden_0"):
         hidden(0)
-    with jax.named_scope("s12_pass_on_3"):
-        pass_on(3)
-    with jax.named_scope("s13_dispatch_5"):
-        dispatch(5)
-    with jax.named_scope("s14_dispatch_6"):
-        dispatch(6)
-    with jax.named_scope("s15_dispatch_7"):
-        dispatch(7)
+    with jax.named_scope("s15_relay_X_3"):
+        relay(X, 3, x_recv, 4)
     with jax.named_scope("s16_relay_X_2"):
         relay(X, 2, x_recv, 4)
-    with jax.named_scope("s17_hidden_relay_0"):
+    with jax.named_scope("s17_pass_on_3"):
+        pass_on(3)
+    with jax.named_scope("s18_take_5"):
+        take(5)
+    with jax.named_scope("s19_hidden_1"):
+        hidden(1)
+    with jax.named_scope("s20_take_4"):
+        take(4)
+    with jax.named_scope("s21_share_queries_"):
+        share_queries()
+    with jax.named_scope("s22_expand_"):
+        expand()
+    with jax.named_scope("s23_hidden_relay_1"):
+        hidden_relay(1)
+    with jax.named_scope("s24_hidden_relay_0"):
         hidden_relay(0)
-    with jax.named_scope("s18_take_3"):
-        take(3)
-    with jax.named_scope("s19_take_4"):
-        take(4)
-    with jax.named_scope("s20_relay_X_3"):
-        relay(X, 3, x_recv, 4)
-    with jax.named_scope("s21_expand_"):
-        expand()
-    with jax.named_scope("s22_relay_X_4"):
+    with jax.named_scope("s25_head_0"):
+        head(0)
+    with jax.named_scope("s26_give_back_0"):
+        give_back(0)
+    with jax.named_scope("s27_relay_X_4"):
         relay(X, 4, x_recv, 4)
-    with jax.named_scope("s23_hidden_1"):
-        hidden(1)
-    with jax.named_scope("s24_head_0"):
-        head(0)
-    with jax.named_scope("s25_take_5"):
-        take(5)
-    with jax.named_scope("s26_load_dd_"):
+    with jax.named_scope("s28_relay_X_5"):
+        relay(X, 5, x_recv, 4)
+    with jax.named_scope("s29_take_6"):
+        take(6)
+    with jax.named_scope("s30_load_dd_"):
         load_d.wait()
         drain(wd.at[pl.ds(0, TP - 1)], one_recv.at[0])
-    with jax.named_scope("s27_down_0"):
+    with jax.named_scope("s31_down_1"):
+        down(1)
+    with jax.named_scope("s32_head_1"):
+        head(1)
+    with jax.named_scope("s33_give_back_1"):
+        give_back(1)
+    with jax.named_scope("s34_down_0"):
         down(0)
-    with jax.named_scope("s28_head_1"):
-        head(1)
-    with jax.named_scope("s29_take_6"):
-        take(6)
-    with jax.named_scope("s30_relay_X_5"):
-        relay(X, 5, x_recv, 4)
-    with jax.named_scope("s31_hidden_relay_1"):
-        hidden_relay(1)
-    with jax.named_scope("s32_head_2"):
-        head(2)
-    with jax.named_scope("s33_take_7"):
-        take(7)
-    with jax.named_scope("s34_relay_X_6"):
-        relay(X, 6, x_recv, 4)
     with jax.named_scope("s35_hidden_2"):
         hidden(2)
-    with jax.named_scope("s36_down_1"):
-        down(1)
-    with jax.named_scope("s37_head_3"):
+    with jax.named_scope("s36_head_2"):
+        head(2)
+    with jax.named_scope("s37_give_back_2"):
+        give_back(2)
+    with jax.named_scope("s38_relay_X_6"):
+        relay(X, 6, x_recv, 4)
+    with jax.named_scope("s39_relay_X_7"):
+        relay(X, 7, x_recv, 4)
+    with jax.named_scope("s40_hidden_relay_2"):
+        hidden_relay(2)
+    with jax.named_scope("s41_head_3"):
         head(3)
-    with jax.named_scope("s38_relay_X_7"):
-        relay(X, 7, x_recv, 4)
-    with jax.named_scope("s39_hidden_relay_2"):
-        hidden_relay(2)
-    with jax.named_scope("s40_give_back_"):
-        give_back()
-    with jax.named_scope("s41_hidden_3"):
+    with jax.named_scope("s42_give_back_3"):
+        give_back(3)
+    with jax.named_scope("s43_give_totals_"):
+        give_totals()
+    with jax.named_scope("s44_hidden_3"):
         hidden(3)
-    with jax.named_scope("s42_down_2"):
+    with jax.named_scope("s45_down_2"):
         down(2)
-    with jax.named_scope("s43_hidden_relay_3"):
+    with jax.named_scope("s46_hidden_relay_3"):
         hidden_relay(3)
-    with jax.named_scope("s44_project_"):
+    with jax.named_scope("s47_project_"):
         project()
-    with jax.named_scope("s45_down_3"):
+    with jax.named_scope("s48_down_3"):
         down(3)
-    with jax.named_scope("s46_finish_mixed_"):
+    with jax.named_scope("s49_finish_mixed_"):
         finish_mixed()
 
     with jax.named_scope("returns"):
@@ -627,7 +640,7 @@
     drain(H.at[pl.ds(0, 2)], send_sem.at[6])
     drain(H.at[0], send_sem.at[7])
     drain(Dn.at[pl.ds(0, slots - cell)], send_sem.at[8])
-    drain(o_in.at[pl.ds(0, J - 1)], send_sem.at[9])
+    drain(o_in.at[:, pl.ds(0, J - 1)], send_sem.at[9])
     drain(t_in.at[pl.ds(0, J - 1)], send_sem.at[10])
     drain(p_in.at[pl.ds(0, TP - 1)], send_sem.at[11])
     drain(m_recv.at[pl.ds(0, TP - 1)], send_sem.at[12])
@@ -741,10 +754,10 @@
                 V(rows, 768),
                 V(4, NZ * rows, 256),
                 V(4, NZ * rows, 256),
-                V(J * rows, 512),
+                V(4, J * rows, VD),
                 F(J * rows, 128),
                 F(J, 8, rows),
-                V(J, rows, 512),
+                V(4, J, rows, VD),
                 F(J, 8, rows),
                 V(rows, D),
                 V(TP, quarter, D),

time: 112 us -> 102 us (0.911)
  Pallas kernels: 107 us -> 97.7 us
    pallas_call x1, Pallas kernels: 107 us -> 97.7 us  [local(): pl.pallas_call(body, name='layer', out_shape=(out, out), in_specs=[hbm, v...]
where the time goes in v2:
time: 102 us
  Pallas kernels  97.7 us (96%)
  local copies, waits for them, and re-layouts  3.14 us (3%)
    pallas_call x1, Pallas kernels, local(): pl.pallas_call(body, name='layer', out_shape=(out, out), in_specs=[hbm, v...  97.7 us
    unnamed x2, local copies, waits for them, and re-layouts  3.14 us

profile of v2, /device:TPU:1, one launch (start us, length us, event | category | flops | bytes accessed | tf_op | source)
XLA Modules:
  0.0 101.5 jit_solution(8979340007196296593)
XLA Ops:
  0.6 97.7 %layer.1 = (bf16[32,2048]{1,0:T(8,128)(2,1)}, bf16[32,2048]{1,0:T(8,128)(2,1)}) custom-call(bf16[128,2048]{1,0:T(8,128)(2,1)} %refs_0_.1, f32[1,2048]{1,0:T(1,128)} %bitcast.8, bf16[2048,768]{1,0:T(8,128)(2,1)} %refs_2_.1, bf16[2048,512]{1,0:T(8,128)(2,1)} %refs_3_.1, bf16[64,2048]{1,0:T(8,128)(2,1)} %bitcast.7, f32[1,512]{1,0:T(1,128)} %bitcast.11, ...), custom_call_target="tpu_custom_call" | custom-call | tf_op jit(solution)/shard_map/layer/pallas_call | solution.py:720
  98.4 1.6 %copy.23 = bf16[32,2048]{1,0:T(8,128)(2,1)} copy(bf16[32,2048]{1,0:T(8,128)(2,1)} %get-tuple-element.4) | data formatting | bytes 262144
  99.9 1.6 %copy.24 = bf16[32,2048]{1,0:T(8,128)(2,1)} copy(bf16[32,2048]{1,0:T(8,128)(2,1)} %get-tuple-element.5) | data formatting | bytes 262144

commit v3 on v2

--- a/solution.py
+++ b/solution.py
@@ -22,6 +22,9 @@
 f32 = jnp.float32
 
 ORDER = (0, 4, 3, 5, 2, 6, 1, 7)
+
+BATCHES = ((0, 1), (2, 3), (4, 5), (6,), (7,))
+DIRECT = (7,)
 
 
 def iota(shape, dim):
@@ -205,7 +208,7 @@
     with jax.named_scope("barrier"):
         pl.semaphore_wait(barrier, E - 1 + TP - 1)
 
-    for step in range(1, TP):
+    def share_down(step):
         peer = lax.rem(t + step, TP)
         send(
             down_weight.at[0, :, pl.ds(pl.multiple_of(peer * width, 128), width)],
@@ -215,6 +218,9 @@
             e,
             peer,
         )
+
+    share_down(1)
+    share_down(TP - 1)
 
     my_rows = pl.ds(pl.multiple_of(e * cell, cell), cell)
 
@@ -269,36 +275,39 @@
         drain(KV.at[across, pl.ds(0, half)], kv_recv.at[0, NZ // 2 - 1])
         drain(KV.at[across, pl.ds(half, half)], kv_recv.at[1, NZ // 2 - 1])
 
-    dispatch(1)
-    load_mix.wait()
-    mix_v[...] = rms(mix_v[...].astype(f32), mix_gain[...]).astype(bf16)
-    load_l.wait()
-    latent = jnp.dot(mix_v[...], lw[...], preferred_element_type=f32)
-    KV[z, :, 0:512] = rms(latent, latent_gain[...]).astype(bf16)
-    load_r.wait()
-    rotary = lax.dot_general(
-        mix_v[...], rw[...], (((1,), (1,)), ((), ())), preferred_element_type=f32
-    )
-    KV[z, :, 512:640] = turned(jnp.concatenate([rotary, rotary], axis=1)).astype(bf16)
-
-    pass_on(0)
-    dispatch(2)
-
-    load_q.wait()
-    queries = jnp.dot(mix_v[...], qw[...], preferred_element_type=f32)
-    low_lanes = lane < 64
-    A = [queries[:, 128 * i : 128 * (i + 1)] for i in range(6)]
-    q_out[:, 0:128] = A[0].astype(bf16)
-    q_out[:, 128:256] = pltpu.roll(jnp.where(low_lanes, A[2], A[1]), 64, 1).astype(bf16)
-    q_out[:, 256:384] = A[3].astype(bf16)
-    q_out[:, 384:512] = pltpu.roll(jnp.where(low_lanes, A[5], A[4]), 64, 1).astype(bf16)
-    q_out[:, 512:640] = turned(jnp.where(low_lanes, A[1], A[2])).astype(bf16)
-    q_out[:, 640:768] = turned(jnp.where(low_lanes, A[4], A[5])).astype(bf16)
-    Q[j] = q_out[...]
+    def own_norm():
+        load_mix.wait()
+        mix_v[...] = rms(mix_v[...].astype(f32), mix_gain[...]).astype(bf16)
+
+    def own_latents():
+        load_l.wait()
+        latent = jnp.dot(mix_v[...], lw[...], preferred_element_type=f32)
+        KV[z, :, 0:512] = rms(latent, latent_gain[...]).astype(bf16)
+        load_r.wait()
+        rotary = lax.dot_general(
+            mix_v[...], rw[...], (((1,), (1,)), ((), ())), preferred_element_type=f32
+        )
+        KV[z, :, 512:640] = turned(jnp.concatenate([rotary, rotary], axis=1)).astype(bf16)
+
+        pass_on(0)
+
     mate = j + 1 - 2 * lax.rem(j, 2)
-    for step in range(2, J, 2):
-        send(Q.at[j], Q.at[j], send_sem.at[2], one_recv.at[1], z * J + lax.rem(j + step, J), t)
-    send(Q.at[j], Q.at[j], send_sem.at[14], one_recv.at[8], z * J + mate, t)
+
+    def own_queries():
+        load_q.wait()
+        queries = jnp.dot(mix_v[...], qw[...], preferred_element_type=f32)
+        low_lanes = lane < 64
+        A = [queries[:, 128 * i : 128 * (i + 1)] for i in range(6)]
+        q_out[:, 0:128] = A[0].astype(bf16)
+        q_out[:, 128:256] = pltpu.roll(jnp.where(low_lanes, A[2], A[1]), 64, 1).astype(bf16)
+        q_out[:, 256:384] = A[3].astype(bf16)
+        q_out[:, 384:512] = pltpu.roll(jnp.where(low_lanes, A[5], A[4]), 64, 1).astype(bf16)
+        q_out[:, 512:640] = turned(jnp.where(low_lanes, A[1], A[2])).astype(bf16)
+        q_out[:, 640:768] = turned(jnp.where(low_lanes, A[4], A[5])).astype(bf16)
+        Q[j] = q_out[...]
+        for step in range(2, J, 2):
+            send(Q.at[j], Q.at[j], send_sem.at[2], one_recv.at[1], z * J + lax.rem(j + step, J), t)
+        send(Q.at[j], Q.at[j], send_sem.at[14], one_recv.at[8], z * J + mate, t)
 
     def share_queries():
         drain(Q.at[pl.ds(0, J // 2 - 1)], one_recv.at[1])
@@ -306,16 +315,17 @@
             from_j = lax.rem(j + step, J)
             send(Q.at[from_j], Q.at[from_j], send_sem.at[14], one_recv.at[8], z * J + mate, t)
 
-    score = route_scores[...]
-    grown = jnp.exp(score - jnp.max(score, axis=0, keepdims=True))
-    share = grown / jnp.sum(grown, axis=0, keepdims=True)
-    gates = jnp.zeros((slots, rows), f32)
-    for k in range(choose):
-        gates = gates + jnp.where(route[k : k + 1, :] == slot_expert, share[k : k + 1, :], 0.0)
-    gates = jnp.transpose(gates * sel[...].astype(f32))
-    gates_hi = gates.astype(bf16)
-    w_hi[...] = gates_hi
-    w_lo[...] = (gates - gates_hi.astype(f32)).astype(bf16)
+    def weigh():
+        score = route_scores[...]
+        grown = jnp.exp(score - jnp.max(score, axis=0, keepdims=True))
+        share = grown / jnp.sum(grown, axis=0, keepdims=True)
+        gates = jnp.zeros((slots, rows), f32)
+        for k in range(choose):
+            gates = gates + jnp.where(route[k : k + 1, :] == slot_expert, share[k : k + 1, :], 0.0)
+        gates = jnp.transpose(gates * sel[...].astype(f32))
+        gates_hi = gates.astype(bf16)
+        w_hi[...] = gates_hi
+        w_lo[...] = (gates - gates_hi.astype(f32)).astype(bf16)
 
     def unit_rows(number):
         source_z = lax.rem(z + ORDER[number], NZ)
@@ -325,12 +335,23 @@
         place = unit_rows(number)
         send(buf.at[t, place], buf.at[t, place], send_sem.at[base_send], sems.at[0, number], e, right)
         send(buf.at[t, place], buf.at[t, place], send_sem.at[base_send], sems.at[1, number], e, left)
+        if buf is H and number in DIRECT:
+            send(
+                buf.at[t, place],
+                buf.at[t, place],
+                send_sem.at[base_send + 1],
+                sems.at[2, number],
+                e,
+                lax.rem(t + 2, TP),
+            )
 
     def relay(buf, number, sems, base_send):
         place = unit_rows(number)
         drain(buf.at[left, place], sems.at[0, number])
         drain(buf.at[right, place], sems.at[1, number])
-        if number % 2 == 0:
+        if buf is H and number in DIRECT:
+            return
+        if number % 2 == 0 or (buf is H and number == 7):
             send(
                 buf.at[left, place],
                 buf.at[left, place],
@@ -361,12 +382,13 @@
             spread(X, number, x_recv, 4)
 
     def hidden(batch):
-        pair = (2 * batch, 2 * batch + 1)
+        pair = BATCHES[batch]
         for number in pair:
             if number > 0:
                 relayed(X, number, x_recv)
-        gate_part = jnp.zeros((2 * unit, gw.shape[1]), f32)
-        up_part = jnp.zeros((2 * unit, gw.shape[1]), f32)
+        tall = len(pair) * unit
+        gate_part = jnp.zeros((tall, gw.shape[1]), f32)
+        up_part = jnp.zeros((tall, gw.shape[1]), f32)
         for part in range(TP):
             block = jnp.concatenate([X[part, unit_rows(number)] for number in pair], axis=0)
             depth = pl.ds(part * width, width)
@@ -381,14 +403,14 @@
             spread(H, number, h_recv, 6)
 
     def hidden_relay(batch):
-        for number in (2 * batch, 2 * batch + 1):
+        for number in BATCHES[batch]:
             relay(H, number, h_recv, 6)
 
     def down(batch):
-        pair = (2 * batch, 2 * batch + 1)
+        pair = BATCHES[batch]
         for number in pair:
             relayed(H, number, h_recv)
-        total = jnp.zeros((2 * unit, width), f32)
+        total = jnp.zeros((len(pair) * unit, width), f32)
         for part in range(TP):
             block = jnp.concatenate([H[part, unit_rows(number)] for number in pair], axis=0)
             total = total + jnp.dot(block, wd[part], preferred_element_type=f32)
@@ -418,26 +440,32 @@
         latents_here()
         load_k.wait()
         load_v.wait()
-        lat = KV[...].reshape(NZ * rows, 640)
+        lat = jnp.concatenate([KV[lax.rem(z + p, NZ)] for p in range(NZ)], axis=0)
         turn = lat[:, 512:640]
         keys = jnp.dot(lat[:, :512], kw[...], preferred_element_type=f32).astype(bf16)
         values = jnp.dot(lat[:, :512], vw[...], preferred_element_type=f32).astype(bf16)
-        low = iota((NZ * rows, 128), 1) < 64
-        zero = jnp.zeros_like(turn)
-        even, odd = jnp.where(low, turn, zero), jnp.where(low, zero, turn)
-        ones = jnp.ones_like(turn)
-        for h in range(4):
-            Kc[h, :, 0:128] = keys[:, 128 * h : 128 * (h + 1)]
-            Kc[h, :, 128:256] = even if h % 2 == 0 else odd
-            Vc[h, :, 0:128] = values[:, 128 * h : 128 * (h + 1)]
-            Vc[h, :, 128:256] = ones
-
-    scale = (NOPE + ROPE) ** (-0.5)
-
-    def head(h):
+        low = iota((rows, 128), 1) < 64
+        zero = jnp.zeros((rows, 128), bf16)
+        for p in range(NZ):
+            here = slice(p * rows, (p + 1) * rows)
+            earlier = z + p >= NZ
+            keep = (lambda v: v) if p == 0 else (lambda v, earlier=earlier: jnp.where(earlier, v, zero))
+            piece = keep(turn[here])
+            even, odd = jnp.where(low, piece, zero), jnp.where(low, zero, piece)
+            ones = keep(jnp.ones((rows, 128), bf16))
+            for h in range(4):
+                Kc[h, here, 0:128] = keep(keys[here, 128 * h : 128 * (h + 1)])
+                Kc[h, here, 128:256] = even if h % 2 == 0 else odd
+                Vc[h, here, 0:128] = keep(values[here, 128 * h : 128 * (h + 1)])
+                Vc[h, here, 128:256] = ones
+
+    scale = (NOPE + ROPE) ** (-0.5) * float(np.log2(np.e))
+
+    def head(part):
+        h, first = part // 2, (part % 2) * (J // 4)
         span = 2 * rows
 
-        @pl.loop(0, J // 2)
+        @pl.loop(first, first + J // 4)
         def _(chunk):
             plain = Q[pl.ds(2 * chunk, 2), :, 128 * h : 128 * (h + 1)].reshape(span, 128)
             pair = 512 + 128 * (h // 2)
@@ -446,10 +474,11 @@
             scores = lax.dot_general(
                 both, Kc[h], (((1,), (1,)), ((), ())), preferred_element_type=f32
             )
-            place = iota((1, NZ * rows), 1)
-            key_place = (place // rows) * (J * rows) + j * rows + place % rows
-            query_place = z * (J * rows) + chunk * span + iota((span, 1), 0)
-            weights = jnp.where(key_place <= query_place, jnp.exp(scores * scale), 0.0).astype(bf16)
+            grown = jnp.exp2(scores * scale)
+            key_place = j * rows + iota((1, rows), 1)
+            query_place = chunk * span + iota((span, 1), 0)
+            near_z = jnp.where(key_place <= query_place, grown[:, :rows], 0.0)
+            weights = jnp.concatenate([near_z.astype(bf16), grown[:, rows:].astype(bf16)], axis=1)
             both_out = jnp.dot(weights, Vc[h], preferred_element_type=f32)
             here = pl.ds(pl.multiple_of(chunk * span, span), span)
             o_out[h, here, :] = both_out[:, :128].astype(bf16)
@@ -510,107 +539,130 @@
             projected = projected + p_in[i].astype(f32)
         mixed_out[...] = rms(projected, out_gain[...]).astype(bf16)
 
-    with jax.named_scope("s00_dispatch_7"):
-        dispatch(7)
-    with jax.named_scope("s01_dispatch_3"):
+    with jax.named_scope("s00_share_down_0"):
+        share_down(2)
+    with jax.named_scope("s01_dispatch_2"):
+        dispatch(2)
+    with jax.named_scope("s02_dispatch_3"):
         dispatch(3)
-    with jax.named_scope("s02_dispatch_4"):
+    with jax.named_scope("s03_dispatch_1"):
+        dispatch(1)
+    with jax.named_scope("s04_own_norm_"):
+        own_norm()
+    with jax.named_scope("s05_own_queries_0"):
+        own_queries()
+    with jax.named_scope("s06_own_latents_0"):
+        own_latents()
+    with jax.named_scope("s07_weigh_0"):
+        weigh()
+    with jax.named_scope("s08_take_3"):
+        take(3)
+    with jax.named_scope("s09_take_2"):
+        take(2)
+    with jax.named_scope("s10_dispatch_5"):
+        dispatch(5)
+    with jax.named_scope("s11_dispatch_6"):
+        dispatch(6)
+    with jax.named_scope("s12_relay_3"):
+        relay(X, 3, x_recv, 4)
+    with jax.named_scope("s13_take_1"):
+        take(1)
+    with jax.named_scope("s14_pass_on_1"):
+        pass_on(1)
+    with jax.named_scope("s15_dispatch_4"):
         dispatch(4)
-    with jax.named_scope("s03_pass_on_1"):
-        pass_on(1)
-    with jax.named_scope("s04_take_1"):
-        take(1)
-    with jax.named_scope("s05_relay_X_1"):
-        relay(X, 1, x_recv, 4)
-    with jax.named_scope("s06_take_7"):
-        take(7)
-    with jax.named_scope("s07_dispatch_6"):
-        dispatch(6)
-    with jax.named_scope("s08_dispatch_5"):
-        dispatch(5)
-    with jax.named_scope("s09_take_0"):
-        take(0)
-    with jax.named_scope("s10_take_2"):
-        take(2)
-    with jax.named_scope("s11_take_3"):
-        take(3)
-    with jax.named_scope("s12_pass_on_2"):
-        pass_on(2)
-    with jax.named_scope("s13_load_gu_"):
+    with jax.named_scope("s16_relay_2"):
+        relay(X, 2, x_recv, 4)
+    with jax.named_scope("s17_take_6"):
+        take(6)
+    with jax.named_scope("s18_take_5"):
+        take(5)
+    with jax.named_scope("s19_load_gu_"):
         load_g.wait()
         load_u.wait()
-    with jax.named_scope("s14_hidden_0"):
+    with jax.named_scope("s20_hidden_1"):
+        hidden(1)
+    with jax.named_scope("s21_relay_1"):
+        relay(X, 1, x_recv, 4)
+    with jax.named_scope("s22_pass_on_2"):
+        pass_on(2)
+    with jax.named_scope("s23_relay_6"):
+        relay(X, 6, x_recv, 4)
+    with jax.named_scope("s24_dispatch_7"):
+        dispatch(7)
+    with jax.named_scope("s25_take_4"):
+        take(4)
+    with jax.named_scope("s26_hidden_relay_1"):
+        hidden_relay(1)
+    with jax.named_scope("s27_take_0"):
+        take(0)
+    with jax.named_scope("s28_pass_on_3"):
+        pass_on(3)
+    with jax.named_scope("s29_share_queries_0"):
+        share_queries()
+    with jax.named_scope("s30_hidden_0"):
         hidden(0)
-    with jax.named_scope("s15_relay_X_3"):
-        relay(X, 3, x_recv, 4)
-    with jax.named_scope("s16_relay_X_2"):
-        relay(X, 2, x_recv, 4)
-    with jax.named_scope("s17_pass_on_3"):
-        pass_on(3)
-    with jax.named_scope("s18_take_5"):
-        take(5)
-    with jax.named_scope("s19_hidden_1"):
-        hidden(1)
-    with jax.named_scope("s20_take_4"):
-        take(4)
-    with jax.named_scope("s21_share_queries_"):
-        share_queries()
-    with jax.named_scope("s22_expand_"):
+    with jax.named_scope("s31_expand_0"):
         expand()
-    with jax.named_scope("s23_hidden_relay_1"):
-        hidden_relay(1)
-    with jax.named_scope("s24_hidden_relay_0"):
-        hidden_relay(0)
-    with jax.named_scope("s25_head_0"):
+    with jax.named_scope("s32_relay_5"):
+        relay(X, 5, x_recv, 4)
+    with jax.named_scope("s33_relay_4"):
+        relay(X, 4, x_recv, 4)
+    with jax.named_scope("s34_head_0"):
         head(0)
-    with jax.named_scope("s26_give_back_0"):
+    with jax.named_scope("s35_head_1"):
+        head(1)
         give_back(0)
-    with jax.named_scope("s27_relay_X_4"):
-        relay(X, 4, x_recv, 4)
-    with jax.named_scope("s28_relay_X_5"):
-        relay(X, 5, x_recv, 4)
-    with jax.named_scope("s29_take_6"):
-        take(6)
-    with jax.named_scope("s30_load_dd_"):
+    with jax.named_scope("s36_take_7"):
+        take(7)
+    with jax.named_scope("s37_load_dd_"):
         load_d.wait()
         drain(wd.at[pl.ds(0, TP - 1)], one_recv.at[0])
-    with jax.named_scope("s31_down_1"):
+    with jax.named_scope("s38_down_1"):
         down(1)
-    with jax.named_scope("s32_head_1"):
-        head(1)
-    with jax.named_scope("s33_give_back_1"):
-        give_back(1)
-    with jax.named_scope("s34_down_0"):
-        down(0)
-    with jax.named_scope("s35_hidden_2"):
-        hidden(2)
-    with jax.named_scope("s36_head_2"):
+    with jax.named_scope("s39_head_2"):
         head(2)
-    with jax.named_scope("s37_give_back_2"):
-        give_back(2)
-    with jax.named_scope("s38_relay_X_6"):
-        relay(X, 6, x_recv, 4)
-    with jax.named_scope("s39_relay_X_7"):
-        relay(X, 7, x_recv, 4)
-    with jax.named_scope("s40_hidden_relay_2"):
-        hidden_relay(2)
+    with jax.named_scope("s40_hidden_relay_0"):
+        hidden_relay(0)
     with jax.named_scope("s41_head_3"):
         head(3)
-    with jax.named_scope("s42_give_back_3"):
+        give_back(1)
+    with jax.named_scope("s42_head_4"):
+        head(4)
+    with jax.named_scope("s43_head_5"):
+        head(5)
+        give_back(2)
+    with jax.named_scope("s44_hidden_2"):
+        hidden(2)
+    with jax.named_scope("s45_relay_7"):
+        relay(X, 7, x_recv, 4)
+    with jax.named_scope("s46_head_6"):
+        head(6)
+    with jax.named_scope("s47_head_7"):
+        head(7)
         give_back(3)
-    with jax.named_scope("s43_give_totals_"):
         give_totals()
-    with jax.named_scope("s44_hidden_3"):
+    with jax.named_scope("s48_down_0"):
+        down(0)
+    with jax.named_scope("s49_hidden_relay_2"):
+        hidden_relay(2)
+    with jax.named_scope("s50_hidden_3"):
         hidden(3)
-    with jax.named_scope("s45_down_2"):
+    with jax.named_scope("s51_hidden_4"):
+        hidden(4)
+    with jax.named_scope("s52_down_2"):
         down(2)
-    with jax.named_scope("s46_hidden_relay_3"):
+    with jax.named_scope("s53_hidden_relay_3"):
         hidden_relay(3)
-    with jax.named_scope("s47_project_"):
+    with jax.named_scope("s54_project_0"):
         project()
-    with jax.named_scope("s48_down_3"):
+    with jax.named_scope("s55_hidden_relay_4"):
+        hidden_relay(4)
+    with jax.named_scope("s56_down_4"):
+        down(4)
+    with jax.named_scope("s57_down_3"):
         down(3)
-    with jax.named_scope("s49_finish_mixed_"):
+    with jax.named_scope("s58_finish_mixed_0"):
         finish_mixed()
 
     with jax.named_scope("returns"):
@@ -716,7 +768,7 @@
         def body(*refs):
             kernel(NZ, J, TP, *refs)
 
-        out = jax.ShapeDtypeStruct((quarter, D), bf16)
+        out = pltpu.VMEM((quarter, D), bf16)
         return pl.pallas_call(
             body,
             name="layer",

time: 102 us -> 92.8 us (0.910)
  Pallas kernels: 97.7 us -> 90.8 us
  local copies, waits for them, and re-layouts: 3.14 us -> 1.31 us
    pallas_call x1, Pallas kernels: 97.7 us -> 90.8 us  [local(): pl.pallas_call(body, name='layer', out_shape=(out, out), in_specs=[hbm, v...]
    unnamed x2, local copies, waits for them, and re-layouts: 3.14 us -> 1.31 us
where the time goes in v3:
time: 92.8 us; the launch traced here: 92.7 us
  Pallas kernels  90.8 us (98%)
  local copies, waits for them, and re-layouts  1.31 us (1%)
    pallas_call x1, Pallas kernels, local(): pl.pallas_call(body, name='layer', out_shape=(out, out), in_specs=[hbm, v...  90.8 us

profile of v3, /device:TPU:1, one launch (start us, length us, event | category | flops | bytes accessed | tf_op | source)
XLA Modules:
  0.0 92.7 jit_solution(9752732167285250318)
XLA Ops:
  0.6 90.8 %layer.1 = (bf16[32,2048]{1,0:T(8,128)(2,1)S(1)}, bf16[32,2048]{1,0:T(8,128)(2,1)S(1)}) custom-call(bf16[128,2048]{1,0:T(8,128)(2,1)} %refs_0_.1, f32[1,2048]{1,0:T(1,128)} %bitcast.8, bf16[2048,768]{1,0:T(8,128)(2,1)} %refs_2_.1, bf16[2048,512]{1,0:T(8,128)(2,1)} %refs_3_.1, bf16[64,2048]{1,0:T(8,128)(2,1)} %bitcast.7, f32[1,512]{1,0:T(1,128)} %bitcast.11, ...), custom_call_target="tpu_custom_call" | custom-call | tf_op jit(solution)/shard_map/layer/pallas_call | solution.py:772
  91.4 0.7 copy.23
  92.1 0.7 copy.24

commit v4 on v3

--- a/solution.py
+++ b/solution.py
@@ -24,7 +24,8 @@
 ORDER = (0, 4, 3, 5, 2, 6, 1, 7)
 
 BATCHES = ((0, 1), (2, 3), (4, 5), (6,), (7,))
-DIRECT = (7,)
+LATE = (6, 7)
+DIRECT = (6, 7)
 
 
 def iota(shape, dim):
@@ -77,6 +78,7 @@
     gw,
     uw,
     wd,
+    dw,
     outg,
     near,
     X,
@@ -135,6 +137,20 @@
             device_id_type=MESH,
         ).start()
 
+    barrier = pltpu.get_barrier_semaphore()
+
+    for dz in (4, 3, 5, 2, 6, 1, 7, 0):
+
+        @pl.loop(1 if dz == 0 else 0, J, unroll=True)
+        def _(step, dz=dz):
+            peer = lax.rem(z + dz, NZ) * J + lax.rem(j + step, J)
+            pl.semaphore_signal(barrier, inc=1, device_id=(peer, t), device_id_type=MESH)
+
+    for step in range(1, TP):
+        pl.semaphore_signal(
+            barrier, inc=1, device_id=(e, lax.rem(t + step, TP)), device_id_type=MESH
+        )
+
     load_ffn = load(ffn_in, ffn_v, 0)
     load_mix = load(mix_in, mix_v, 1)
     load_q = load(query_weight, qw, 2)
@@ -147,21 +163,8 @@
     load_d = load(
         down_weight.at[0, :, pl.ds(pl.multiple_of(t * width, 128), width)], wd.at[t], 9
     )
+    load_w = load(down_weight.at[0], dw, 11)
     load_o = load(output_weight, ow, 10)
-
-    barrier = pltpu.get_barrier_semaphore()
-
-    for dz in (4, 3, 5, 2, 6, 1, 7, 0):
-
-        @pl.loop(1 if dz == 0 else 0, J)
-        def _(step, dz=dz):
-            peer = lax.rem(z + dz, NZ) * J + lax.rem(j + step, J)
-            pl.semaphore_signal(barrier, inc=1, device_id=(peer, t), device_id_type=MESH)
-
-    for step in range(1, TP):
-        pl.semaphore_signal(
-            barrier, inc=1, device_id=(e, lax.rem(t + step, TP)), device_id_type=MESH
-        )
 
     slots = outg.shape[0]
     blocks = rows // QB
@@ -205,13 +208,14 @@
         partner = jnp.where(first_half, pltpu.roll(v, 96, 1), pltpu.roll(v, 32, 1))
         return v * cosine + partner * sine
 
+    load_w.wait()
     with jax.named_scope("barrier"):
         pl.semaphore_wait(barrier, E - 1 + TP - 1)
 
     def share_down(step):
         peer = lax.rem(t + step, TP)
         send(
-            down_weight.at[0, :, pl.ds(pl.multiple_of(peer * width, 128), width)],
+            dw.at[:, pl.ds(pl.multiple_of(peer * width, 128), width)],
             wd.at[t],
             send_sem.at[1],
             one_recv.at[0],
@@ -421,13 +425,13 @@
             source_z = lax.rem(z + ORDER[number], NZ)
 
             @pl.loop(1 if ORDER[number] == 0 else 0, J)
-            def _(step, source_z=source_z):
+            def _(step, source_z=source_z, back=9 if number in LATE else 3):
                 source = source_z * J + lax.rem(j + step, J)
                 send(
                     Dn.at[pl.ds(pl.multiple_of(source * cell, cell), cell)],
                     R.at[my_rows],
                     send_sem.at[8],
-                    one_recv.at[3],
+                    one_recv.at[back],
                     source,
                     t,
                 )
@@ -462,32 +466,29 @@
     scale = (NOPE + ROPE) ** (-0.5) * float(np.log2(np.e))
 
     def head(part):
-        h, first = part // 2, (part % 2) * (J // 4)
-        span = 2 * rows
-
-        @pl.loop(first, first + J // 4)
-        def _(chunk):
-            plain = Q[pl.ds(2 * chunk, 2), :, 128 * h : 128 * (h + 1)].reshape(span, 128)
-            pair = 512 + 128 * (h // 2)
-            turn = Q[pl.ds(2 * chunk, 2), :, pair : pair + 128].reshape(span, 128)
-            both = jnp.concatenate([plain, turn], axis=1)
-            scores = lax.dot_general(
-                both, Kc[h], (((1,), (1,)), ((), ())), preferred_element_type=f32
-            )
-            grown = jnp.exp2(scores * scale)
-            key_place = j * rows + iota((1, rows), 1)
-            query_place = chunk * span + iota((span, 1), 0)
-            near_z = jnp.where(key_place <= query_place, grown[:, :rows], 0.0)
-            weights = jnp.concatenate([near_z.astype(bf16), grown[:, rows:].astype(bf16)], axis=1)
-            both_out = jnp.dot(weights, Vc[h], preferred_element_type=f32)
-            here = pl.ds(pl.multiple_of(chunk * span, span), span)
-            o_out[h, here, :] = both_out[:, :128].astype(bf16)
-            sums = both_out[:, 128:]
-            if h == 0:
-                t_out[here, :] = sums
-            else:
-                lanes = iota((span, 128), 1)
-                t_out[here, :] = jnp.where(lanes // 32 == h, sums, t_out[here, :])
+        h, chunk = part // 2, part % 2
+        span = (J // 2) * rows
+        plain = Q[chunk * (J // 2) : (chunk + 1) * (J // 2), :, 128 * h : 128 * (h + 1)].reshape(span, 128)
+        pair = 512 + 128 * (h // 2)
+        turn = Q[chunk * (J // 2) : (chunk + 1) * (J // 2), :, pair : pair + 128].reshape(span, 128)
+        both = jnp.concatenate([plain, turn], axis=1)
+        scores = lax.dot_general(
+            both, Kc[h], (((1,), (1,)), ((), ())), preferred_element_type=f32
+        )
+        grown = jnp.exp2(scores * scale)
+        key_place = j * rows + iota((1, rows), 1)
+        query_place = chunk * span + iota((span, 1), 0)
+        near_z = jnp.where(key_place <= query_place, grown[:, :rows], 0.0)
+        weights = jnp.concatenate([near_z.astype(bf16), grown[:, rows:].astype(bf16)], axis=1)
+        both_out = jnp.dot(weights, Vc[h], preferred_element_type=f32)
+        here = slice(chunk * span, (chunk + 1) * span)
+        o_out[h, here, :] = both_out[:, :128].astype(bf16)
+        sums = both_out[:, 128:]
+        if h == 0:
+            t_out[here, :] = sums
+        else:
+            lanes = iota((span, 128), 1)
+            t_out[here, :] = jnp.where(lanes // 32 == h, sums, t_out[here, :])
 
     back_order = (4, 2, 6, 3, 5, 1, 7)
 
@@ -539,91 +540,102 @@
             projected = projected + p_in[i].astype(f32)
         mixed_out[...] = rms(projected, out_gain[...]).astype(bf16)
 
+    def add_up(total, numbers, back):
+        count = len(numbers) * unit - (cell if 0 in numbers else 0)
+        with jax.named_scope("returns"):
+            drain(R.at[pl.ds(0, count)], one_recv.at[back])
+        for number in numbers:
+            from_z = lax.rem(z + NZ - ORDER[number], NZ)
+            place = pl.ds(pl.multiple_of(from_z * unit, unit), unit)
+            total = total + jnp.dot(w_hi[:, place], R[place, :], preferred_element_type=f32)
+            total = total + jnp.dot(w_lo[:, place], R[place, :], preferred_element_type=f32)
+        return total
+
     with jax.named_scope("s00_share_down_0"):
         share_down(2)
-    with jax.named_scope("s01_dispatch_2"):
-        dispatch(2)
+    with jax.named_scope("s01_dispatch_6"):
+        dispatch(6)
     with jax.named_scope("s02_dispatch_3"):
         dispatch(3)
-    with jax.named_scope("s03_dispatch_1"):
-        dispatch(1)
-    with jax.named_scope("s04_own_norm_"):
+    with jax.named_scope("s03_dispatch_5"):
+        dispatch(5)
+    with jax.named_scope("s04_dispatch_2"):
+        dispatch(2)
+    with jax.named_scope("s05_own_norm_"):
         own_norm()
-    with jax.named_scope("s05_own_queries_0"):
-        own_queries()
     with jax.named_scope("s06_own_latents_0"):
         own_latents()
-    with jax.named_scope("s07_weigh_0"):
-        weigh()
-    with jax.named_scope("s08_take_3"):
+    with jax.named_scope("s07_take_6"):
+        take(6)
+    with jax.named_scope("s08_dispatch_4"):
+        dispatch(4)
+    with jax.named_scope("s09_own_queries_0"):
+        own_queries()
+    with jax.named_scope("s10_take_3"):
         take(3)
-    with jax.named_scope("s09_take_2"):
+    with jax.named_scope("s11_take_2"):
         take(2)
-    with jax.named_scope("s10_dispatch_5"):
-        dispatch(5)
-    with jax.named_scope("s11_dispatch_6"):
-        dispatch(6)
-    with jax.named_scope("s12_relay_3"):
+    with jax.named_scope("s12_take_5"):
+        take(5)
+    with jax.named_scope("s13_pass_on_1"):
+        pass_on(1)
+    with jax.named_scope("s14_relay_3"):
         relay(X, 3, x_recv, 4)
-    with jax.named_scope("s13_take_1"):
-        take(1)
-    with jax.named_scope("s14_pass_on_1"):
-        pass_on(1)
-    with jax.named_scope("s15_dispatch_4"):
-        dispatch(4)
-    with jax.named_scope("s16_relay_2"):
+    with jax.named_scope("s15_relay_2"):
         relay(X, 2, x_recv, 4)
-    with jax.named_scope("s17_take_6"):
-        take(6)
-    with jax.named_scope("s18_take_5"):
-        take(5)
-    with jax.named_scope("s19_load_gu_"):
+    with jax.named_scope("s16_dispatch_1"):
+        dispatch(1)
+    with jax.named_scope("s17_take_4"):
+        take(4)
+    with jax.named_scope("s18_share_queries_0"):
+        share_queries()
+    with jax.named_scope("s19_pass_on_2"):
+        pass_on(2)
+    with jax.named_scope("s20_load_gu_"):
         load_g.wait()
         load_u.wait()
-    with jax.named_scope("s20_hidden_1"):
+    with jax.named_scope("s21_hidden_1"):
         hidden(1)
-    with jax.named_scope("s21_relay_1"):
-        relay(X, 1, x_recv, 4)
-    with jax.named_scope("s22_pass_on_2"):
-        pass_on(2)
-    with jax.named_scope("s23_relay_6"):
-        relay(X, 6, x_recv, 4)
+    with jax.named_scope("s22_relay_4"):
+        relay(X, 4, x_recv, 4)
+    with jax.named_scope("s23_relay_5"):
+        relay(X, 5, x_recv, 4)
     with jax.named_scope("s24_dispatch_7"):
         dispatch(7)
-    with jax.named_scope("s25_take_4"):
-        take(4)
+    with jax.named_scope("s25_weigh_0"):
+        weigh()
     with jax.named_scope("s26_hidden_relay_1"):
         hidden_relay(1)
-    with jax.named_scope("s27_take_0"):
-        take(0)
-    with jax.named_scope("s28_pass_on_3"):
+    with jax.named_scope("s27_pass_on_3"):
         pass_on(3)
-    with jax.named_scope("s29_share_queries_0"):
-        share_queries()
-    with jax.named_scope("s30_hidden_0"):
-        hidden(0)
-    with jax.named_scope("s31_expand_0"):
+    with jax.named_scope("s28_take_1"):
+        take(1)
+    with jax.named_scope("s29_hidden_2"):
+        hidden(2)
+    with jax.named_scope("s30_load_dd_"):
+        load_d.wait()
+        drain(wd.at[pl.ds(0, TP - 1)], one_recv.at[0])
+    with jax.named_scope("s31_down_1"):
+        down(1)
+    with jax.named_scope("s32_expand_0"):
         expand()
-    with jax.named_scope("s32_relay_5"):
-        relay(X, 5, x_recv, 4)
-    with jax.named_scope("s33_relay_4"):
-        relay(X, 4, x_recv, 4)
-    with jax.named_scope("s34_head_0"):
+    with jax.named_scope("s33_relay_6"):
+        relay(X, 6, x_recv, 4)
+    with jax.named_scope("s34_relay_1"):
+        relay(X, 1, x_recv, 4)
+    with jax.named_scope("s35_head_0"):
         head(0)
-    with jax.named_scope("s35_head_1"):
+    with jax.named_scope("s36_head_1"):
         head(1)
         give_back(0)
-    with jax.named_scope("s36_take_7"):
+    with jax.named_scope("s37_head_2"):
+        head(2)
+    with jax.named_scope("s38_hidden_relay_2"):
+        hidden_relay(2)
+    with jax.named_scope("s39_take_0"):
+        take(0)
+    with jax.named_scope("s40_take_7"):
         take(7)
-    with jax.named_scope("s37_load_dd_"):
-        load_d.wait()
-        drain(wd.at[pl.ds(0, TP - 1)], one_recv.at[0])
-    with jax.named_scope("s38_down_1"):
-        down(1)
-    with jax.named_scope("s39_head_2"):
-        head(2)
-    with jax.named_scope("s40_hidden_relay_0"):
-        hidden_relay(0)
     with jax.named_scope("s41_head_3"):
         head(3)
         give_back(1)
@@ -632,43 +644,42 @@
     with jax.named_scope("s43_head_5"):
         head(5)
         give_back(2)
-    with jax.named_scope("s44_hidden_2"):
-        hidden(2)
-    with jax.named_scope("s45_relay_7"):
+    with jax.named_scope("s44_hidden_0"):
+        hidden(0)
+    with jax.named_scope("s45_head_6"):
+        head(6)
+    with jax.named_scope("s46_relay_7"):
         relay(X, 7, x_recv, 4)
-    with jax.named_scope("s46_head_6"):
-        head(6)
     with jax.named_scope("s47_head_7"):
         head(7)
         give_back(3)
         give_totals()
-    with jax.named_scope("s48_down_0"):
-        down(0)
-    with jax.named_scope("s49_hidden_relay_2"):
-        hidden_relay(2)
+    with jax.named_scope("s48_down_2"):
+        down(2)
+    with jax.named_scope("s49_hidden_relay_0"):
+        hidden_relay(0)
     with jax.named_scope("s50_hidden_3"):
         hidden(3)
     with jax.named_scope("s51_hidden_4"):
         hidden(4)
-    with jax.named_scope("s52_down_2"):
-        down(2)
-    with jax.named_scope("s53_hidden_relay_3"):
+    with jax.named_scope("s52_down_0"):
+        down(0)
+    with jax.named_scope("s53_project_0"):
+        project()
+    with jax.named_scope("s54_hidden_relay_3"):
         hidden_relay(3)
-    with jax.named_scope("s54_project_0"):
-        project()
-    with jax.named_scope("s55_hidden_relay_4"):
+    with jax.named_scope("s55_down_3"):
+        down(3)
+    with jax.named_scope("s56_hidden_relay_4"):
         hidden_relay(4)
-    with jax.named_scope("s56_down_4"):
+    with jax.named_scope("s57_down_4"):
         down(4)
-    with jax.named_scope("s57_down_3"):
-        down(3)
+    total = jnp.zeros((rows, width), f32)
+    total = add_up(total, tuple(n for n in range(NZ) if n not in LATE), 3)
     with jax.named_scope("s58_finish_mixed_0"):
         finish_mixed()
 
-    with jax.named_scope("returns"):
-        drain(R.at[pl.ds(0, slots - cell)], one_recv.at[3])
-    total = jnp.dot(w_hi[...], R[...], preferred_element_type=f32)
-    total = total + jnp.dot(w_lo[...], R[...], preferred_element_type=f32)
+    total = add_up(total, LATE, 9)
     m_send[...] = total.astype(bf16)
     for step in range(1, TP):
         peer = lax.rem(t + step, TP)
@@ -790,6 +801,7 @@
                 V(D, unit),
                 V(D, unit),
                 V(TP, unit, width),
+                V(unit, D),
                 V(slots, width),
                 V(TP, J * cell, width),
                 V(TP, slots, width),
@@ -813,12 +825,12 @@
                 F(J, 8, rows),
                 V(rows, D),
                 V(TP, quarter, D),
-                S((11,)),
+                S((12,)),
                 S((8,)),
                 S((3, 8)),
                 S((3, 8)),
                 S((2, NZ // 2)),
-                S((9,)),
+                S((10,)),
                 S((15,)),
             ],
             compiler_params=pltpu.CompilerParams(

time: 92.8 us -> 90.5 us (0.975)
  Pallas kernels: 90.8 us -> 88.5 us
    pallas_call x1, Pallas kernels: 90.8 us -> 88.5 us  [local(): pl.pallas_call(body, name='layer', out_shape=(out, out), in_specs=[hbm, v...]
where the time goes in v4:
time: 90.5 us; the launch traced here: 90.4 us
  Pallas kernels  88.5 us (98%)
  local copies, waits for them, and re-layouts  1.31 us (1%)
    pallas_call x1, Pallas kernels, local(): pl.pallas_call(body, name='layer', out_shape=(out, out), in_specs=[hbm, v...  88.5 us

profile of v4, /device:TPU:1, one launch (start us, length us, event | category | flops | bytes accessed | tf_op | source)
XLA Modules:
  0.0 90.4 jit_solution(3237739208300666383)
XLA Ops:
  0.6 88.5 %layer.1 = (bf16[32,2048]{1,0:T(8,128)(2,1)S(1)}, bf16[32,2048]{1,0:T(8,128)(2,1)S(1)}) custom-call(bf16[128,2048]{1,0:T(8,128)(2,1)} %refs_0_.1, f32[1,2048]{1,0:T(1,128)} %bitcast.8, bf16[2048,768]{1,0:T(8,128)(2,1)} %refs_2_.1, bf16[2048,512]{1,0:T(8,128)(2,1)} %refs_3_.1, bf16[64,2048]{1,0:T(8,128)(2,1)} %bitcast.7, f32[1,512]{1,0:T(1,128)} %bitcast.11, ...), custom_call_target="tpu_custom_call" | custom-call | tf_op jit(solution)/shard_map/layer/pallas_call | solution.py:783
  89.1 0.7 copy.23
  89.8 0.7 copy.24

commit v5 on v4

--- a/solution.py
+++ b/solution.py
@@ -137,6 +137,9 @@
             device_id_type=MESH,
         ).start()
 
+    load_ffn = load(ffn_in, ffn_v, 0)
+    load_w = load(down_weight.at[0], dw, 11)
+
     barrier = pltpu.get_barrier_semaphore()
 
     for dz in (4, 3, 5, 2, 6, 1, 7, 0):
@@ -151,20 +154,6 @@
             barrier, inc=1, device_id=(e, lax.rem(t + step, TP)), device_id_type=MESH
         )
 
-    load_ffn = load(ffn_in, ffn_v, 0)
-    load_mix = load(mix_in, mix_v, 1)
-    load_q = load(query_weight, qw, 2)
-    load_l = load(latent_weight, lw, 3)
-    load_r = load(rotary_weight, rw, 4)
-    load_k = load(key_weight, kw, 5)
-    load_v = load(value_weight, vw, 6)
-    load_g = load(gate_weight.at[0], gw, 7)
-    load_u = load(up_weight.at[0], uw, 8)
-    load_d = load(
-        down_weight.at[0, :, pl.ds(pl.multiple_of(t * width, 128), width)], wd.at[t], 9
-    )
-    load_w = load(down_weight.at[0], dw, 11)
-    load_o = load(output_weight, ow, 10)
 
     slots = outg.shape[0]
     blocks = rows // QB
@@ -186,6 +175,18 @@
     sel[...] = picked.astype(bf16)
 
     load_ffn.wait()
+    load_mix = load(mix_in, mix_v, 1)
+    load_q = load(query_weight, qw, 2)
+    load_l = load(latent_weight, lw, 3)
+    load_r = load(rotary_weight, rw, 4)
+    load_k = load(key_weight, kw, 5)
+    load_v = load(value_weight, vw, 6)
+    load_g = load(gate_weight.at[0], gw, 7)
+    load_u = load(up_weight.at[0], uw, 8)
+    load_d = load(
+        down_weight.at[0, :, pl.ds(pl.multiple_of(t * width, 128), width)], wd.at[t], 9
+    )
+    load_o = load(output_weight, ow, 10)
     ffn_v[...] = rms(ffn_v[...].astype(f32), ffn_gain[...]).astype(bf16)
     columns = pl.ds(pl.multiple_of(t * width, 128), width)
     outg[...] = jnp.dot(sel[...], ffn_v[:, columns], preferred_element_type=f32).astype(bf16)
@@ -355,7 +356,7 @@
         drain(buf.at[right, place], sems.at[1, number])
         if buf is H and number in DIRECT:
             return
-        if number % 2 == 0 or (buf is H and number == 7):
+        if number % 2 == 0 or (buf is H and number in (1, 7)):
             send(
                 buf.at[left, place],
                 buf.at[left, place],
@@ -510,6 +511,7 @@
         t_in[j] = t_row[j]
 
     quarter = rows // TP
+    far_first = sorted(range(1, TP), key=lambda step: -min(step, TP - step))
 
     def project():
         drain(o_in.at[:, pl.ds(0, J - 1)], one_recv.at[4])
@@ -527,7 +529,7 @@
             heads.append((osum / tsum[:, h : h + 1]).astype(bf16))
         attended = jnp.concatenate(heads, axis=1)
         p_out[...] = jnp.dot(attended, ow[...], preferred_element_type=f32).astype(bf16)
-        for step in range(1, TP):
+        for step in far_first:
             peer = lax.rem(t + step, TP)
             place = pl.ds(pl.multiple_of(peer * quarter, quarter), quarter)
             send(p_out.at[place], p_in.at[t], send_sem.at[11], one_recv.at[6], e, peer)
@@ -648,12 +650,12 @@
         hidden(0)
     with jax.named_scope("s45_head_6"):
         head(6)
-    with jax.named_scope("s46_relay_7"):
-        relay(X, 7, x_recv, 4)
     with jax.named_scope("s47_head_7"):
         head(7)
         give_back(3)
         give_totals()
+    with jax.named_scope("s46_relay_7"):
+        relay(X, 7, x_recv, 4)
     with jax.named_scope("s48_down_2"):
         down(2)
     with jax.named_scope("s49_hidden_relay_0"):
@@ -676,16 +678,16 @@
         down(4)
     total = jnp.zeros((rows, width), f32)
     total = add_up(total, tuple(n for n in range(NZ) if n not in LATE), 3)
-    with jax.named_scope("s58_finish_mixed_0"):
-        finish_mixed()
 
     total = add_up(total, LATE, 9)
     m_send[...] = total.astype(bf16)
-    for step in range(1, TP):
+    for step in far_first:
         peer = lax.rem(t + step, TP)
         place = pl.ds(pl.multiple_of(peer * quarter, quarter), quarter)
         send(m_send.at[place], m_recv.at[t], send_sem.at[12], one_recv.at[7], e, peer)
     m_recv[t] = m_send[pl.ds(pl.multiple_of(t * quarter, quarter), quarter), :]
+    with jax.named_scope("s58_finish_mixed_0"):
+        finish_mixed()
     with jax.named_scope("last"):
         drain(m_recv.at[pl.ds(0, TP - 1)], one_recv.at[7])
     for i in range(TP):

time: 90.5 us -> 89.5 us (0.989)
  Pallas kernels: 88.5 us -> 87.2 us
    pallas_call x1, Pallas kernels: 88.5 us -> 87.2 us  [local(): pl.pallas_call(body, name='layer', out_shape=(out, out), in_specs=[hbm, v...]
where the time goes in v5:
time: 89.5 us; the launch traced here: 89.2 us
  Pallas kernels  87.2 us (97%)
  local copies, waits for them, and re-layouts  1.31 us (1%)
    pallas_call x1, Pallas kernels, local(): pl.pallas_call(body, name='layer', out_shape=(out, out), in_specs=[hbm, v...  87.2 us

profile of v5, /device:TPU:1, one launch (start us, length us, event | category | flops | bytes accessed | tf_op | source)
XLA Modules:
  0.0 89.2 jit_solution(7541932663336644086)
XLA Ops:
  0.6 87.2 %layer.1 = (bf16[32,2048]{1,0:T(8,128)(2,1)S(1)}, bf16[32,2048]{1,0:T(8,128)(2,1)S(1)}) custom-call(bf16[128,2048]{1,0:T(8,128)(2,1)} %refs_0_.1, f32[1,2048]{1,0:T(1,128)} %bitcast.8, bf16[2048,768]{1,0:T(8,128)(2,1)} %refs_2_.1, bf16[2048,512]{1,0:T(8,128)(2,1)} %refs_3_.1, bf16[64,2048]{1,0:T(8,128)(2,1)} %bitcast.7, f32[1,512]{1,0:T(1,128)} %bitcast.11, ...), custom_call_target="tpu_custom_call" | custom-call | tf_op jit(solution)/shard_map/layer/pallas_call | solution.py:785
  87.9 0.7 copy.23
  88.5 0.7 copy.24

commit v6 on v5

--- a/solution.py
+++ b/solution.py
@@ -567,12 +567,12 @@
         own_norm()
     with jax.named_scope("s06_own_latents_0"):
         own_latents()
+    with jax.named_scope("s09_own_queries_0"):
+        own_queries()
     with jax.named_scope("s07_take_6"):
         take(6)
     with jax.named_scope("s08_dispatch_4"):
         dispatch(4)
-    with jax.named_scope("s09_own_queries_0"):
-        own_queries()
     with jax.named_scope("s10_take_3"):
         take(3)
     with jax.named_scope("s11_take_2"):

time: 89.5 us -> 89.6 us (level)
  no operation moved by 1% of the time
where the time goes in v6:
time: 89.6 us; the launch traced here: 89.5 us
  Pallas kernels  87.5 us (98%)
  local copies, waits for them, and re-layouts  1.31 us (1%)
    pallas_call x1, Pallas kernels, local(): pl.pallas_call(body, name='layer', out_shape=(out, out), in_specs=[hbm, v...  87.5 us

profile of v6, /device:TPU:1, one launch (start us, length us, event | category | flops | bytes accessed | tf_op | source)
XLA Modules:
  0.0 89.5 jit_solution(14409072598709988739)
XLA Ops:
  0.6 87.5 %layer.1 = (bf16[32,2048]{1,0:T(8,128)(2,1)S(1)}, bf16[32,2048]{1,0:T(8,128)(2,1)S(1)}) custom-call(bf16[128,2048]{1,0:T(8,128)(2,1)} %refs_0_.1, f32[1,2048]{1,0:T(1,128)} %bitcast.8, bf16[2048,768]{1,0:T(8,128)(2,1)} %refs_2_.1, bf16[2048,512]{1,0:T(8,128)(2,1)} %refs_3_.1, bf16[64,2048]{1,0:T(8,128)(2,1)} %bitcast.7, f32[1,512]{1,0:T(1,128)} %bitcast.11, ...), custom_call_target="tpu_custom_call" | custom-call | tf_op jit(solution)/shard_map/layer/pallas_call | solution.py:785
  88.2 0.7 copy.23
  88.9 0.7 copy.24
